TPU v7x, 32 devices: a whole 2x2x4 slice. The times are simulated.
32 devices in a mesh: sp: 8 (over z, y), dp: 4 (over x, core).
Axes of the slice: x: 2, y: 2, z: 4, core: 2. Of those that a mesh axis runs over, the one named last changes fastest.
Arguments:
- queries: bfloat16 [4, 1024, 16, 128], P('dp', 'sp'), may hold values from -7 to 7
- key_vectors: bfloat16 [4, 1024, 16, 128], P('dp', 'sp'), may hold values from -6 to 6
- value_vectors: bfloat16 [4, 1024, 16, 128], P('dp', 'sp'), may hold values from -6 to 6
- head_lambda: float32 [16], P('sp'), may hold values from 0.3 to 0.8
- head_gain: float32 [128], replicated, may hold values from 0.1 to 1.9
- residual: bfloat16 [4, 1024, 2048], P('dp', 'sp'), may hold values from -6 to 6
- out_weight: bfloat16 [2048, 2048], replicated, may hold values from -0.125 to 0.125
- mix_gain: float32 [2048], replicated, may hold values from 0.1 to 1.9
- pre_gain: float32 [2048], replicated, may hold values from 0.1 to 1.9
- post_gain: float32 [2048], replicated, may hold values from 0.1 to 1.9
- routes: int32 [4, 1024, 4], P('dp', 'sp'), may hold values from 0 to 31, all different within a row; in each aligned block of 128 rows (0 to 127, 128 to 255, ..., all dimensions but the last counted through in order) at most 24 rows name the same one
- route_weights: float32 [4, 1024, 4], P('dp', 'sp'), may hold values from 0.25 to 1
- expert_gate: bfloat16 [32, 2048, 512], P(('sp', 'dp')), may hold values from -0.125 to 0.125
- expert_up: bfloat16 [32, 2048, 512], P(('sp', 'dp')), may hold values from -0.125 to 0.125
- expert_down: bfloat16 [32, 512, 2048], P(('sp', 'dp')), may hold values from -0.25 to 0.25
- shared_gate: bfloat16 [2048, 512], replicated, may hold values from -0.125 to 0.125
- shared_up: bfloat16 [2048, 512], replicated, may hold values from -0.125 to 0.125
- shared_down: bfloat16 [512, 2048], replicated, may hold values from -0.25 to 0.25
Outputs:
- output: bfloat16 [4, 1024, 2048], P('dp', 'sp')
Inputs may be any that keep to these rules, and one draw needn't show every extreme that they name: `routes`: among the tokens of one device (aligned blocks of 128 positions), no expert is named more than 24 times; in some block some expert is named exactly 24 times. Each token names 4 different experts.
All inputs are finite; a program needn't handle non-finite values.
Results may differ from a plain program's by a relative error of at most 0.0075.
Values may be sent and summed in bfloat16 or wider, within the bound.
A program may use at most 128 MiB of HBM per device.

v0:
```python
import functools

import jax
import jax.numpy as jnp
from jax import lax
from jax.experimental import pallas as pl
from jax.experimental.pallas import tpu as pltpu
from jax.sharding import PartitionSpec as P

epsilon = 1e-06
MESH = pl.DeviceIdType.MESH
VMEM = pl.BlockSpec(memory_space=pltpu.VMEM)


def rms_scale(values_in, gain):
    return (
        values_in
        * lax.rsqrt(jnp.mean(values_in * values_in, axis=-1, keepdims=True) + epsilon)
        * gain
    )


def feed_forward(rows, gate_w, up_w, down_w):
    gate_val = jnp.dot(rows, gate_w, preferred_element_type=jnp.float32)
    up_val = jnp.dot(rows, up_w, preferred_element_type=jnp.float32)
    hidden = (jax.nn.silu(gate_val) * up_val).astype(jnp.bfloat16)
    return jnp.dot(hidden, down_w, preferred_element_type=jnp.float32).astype(jnp.bfloat16)


def columns_of(index, width):
    return pl.ds(pl.multiple_of(index * width, width), width)


def line_barrier(n, me):
    barrier = pltpu.get_barrier_semaphore()

    def greet(off, carry):
        pl.semaphore_signal(
            barrier, inc=1, device_id={"sp": lax.rem(me + off, n)}, device_id_type=MESH
        )
        return carry

    lax.fori_loop(1, n, greet, 0)
    pl.semaphore_wait(barrier, n - 1)


def to_heads_kernel(
    n,
    q_ref,
    k_ref,
    v_ref,
    side_ref,
    qo_ref,
    ko_ref,
    vo_ref,
    side_out,
    send_sem,
    recv_sem,
    own_sem,
    side_send,
    side_recv,
):
    me = lax.axis_index("sp")
    width = qo_ref.shape[2]
    pairs = ((q_ref, qo_ref), (k_ref, ko_ref), (v_ref, vo_ref))
    line_barrier(n, me)

    def copy(which, off):
        source, target = pairs[which]
        dst = lax.rem(me + off, n)
        return pltpu.make_async_remote_copy(
            src_ref=source.at[:, columns_of(dst, width)],
            dst_ref=target.at[me],
            send_sem=send_sem.at[which, off],
            recv_sem=recv_sem.at[which, off],
            device_id={"sp": dst},
            device_id_type=MESH,
        )

    def own(which):
        source, target = pairs[which]
        return pltpu.make_async_copy(
            source.at[:, columns_of(me, width)], target.at[me], own_sem.at[which]
        )

    def start(off, carry):
        for which in range(3):
            copy(which, off).start()
        return carry

    def finish(off, carry):
        for which in range(3):
            copy(which, off).wait()
        return carry

    side = pltpu.make_async_remote_copy(
        src_ref=side_ref,
        dst_ref=side_out,
        send_sem=side_send,
        recv_sem=side_recv,
        device_id={"sp": lax.rem(me + n // 2, n)},
        device_id_type=MESH,
    )
    lax.fori_loop(1, n, start, 0)
    side.start()
    for which in range(3):
        own(which).start()
    for which in range(3):
        own(which).wait()
    lax.fori_loop(1, n, finish, 0)
    side.wait()


def to_heads(n, q, k, v, side):
    tok, model = q.shape
    width = model // n
    out = jax.ShapeDtypeStruct((n, tok, width), q.dtype)
    return pl.pallas_call(
        functools.partial(to_heads_kernel, n),
        out_shape=[out] * 3 + [jax.ShapeDtypeStruct(side.shape, side.dtype)],
        in_specs=[VMEM] * 4,
        out_specs=[VMEM] * 4,
        scratch_shapes=[
            pltpu.SemaphoreType.DMA((3, n)),
            pltpu.SemaphoreType.DMA((3, n)),
            pltpu.SemaphoreType.DMA((3,)),
            pltpu.SemaphoreType.DMA,
            pltpu.SemaphoreType.DMA,
        ],
        compiler_params=pltpu.CompilerParams(
            collective_id=0, has_side_effects=True, vmem_limit_bytes=32 * 2**20
        ),
    )(q, k, v, side)


def to_tokens_kernel(n, a_ref, o_ref, send_sem, recv_sem, own_sem):
    me = lax.axis_index("sp")
    width = a_ref.shape[2]
    line_barrier(n, me)

    def copy(off):
        dst = lax.rem(me + off, n)
        return pltpu.make_async_remote_copy(
            src_ref=a_ref.at[dst],
            dst_ref=o_ref.at[:, columns_of(me, width)],
            send_sem=send_sem.at[off],
            recv_sem=recv_sem.at[off],
            device_id={"sp": dst},
            device_id_type=MESH,
        )

    def start(off, carry):
        copy(off).start()
        return carry

    def finish(off, carry):
        copy(off).wait()
        return carry

    lax.fori_loop(1, n, start, 0)
    own = pltpu.make_async_copy(a_ref.at[me], o_ref.at[:, columns_of(me, width)], own_sem)
    own.start()
    own.wait()
    lax.fori_loop(1, n, finish, 0)


def to_tokens(n, attended):
    _, tok, width = attended.shape
    return pl.pallas_call(
        functools.partial(to_tokens_kernel, n),
        out_shape=jax.ShapeDtypeStruct((tok, n * width), attended.dtype),
        in_specs=[VMEM],
        out_specs=VMEM,
        scratch_shapes=[
            pltpu.SemaphoreType.DMA((n,)),
            pltpu.SemaphoreType.DMA((n,)),
            pltpu.SemaphoreType.DMA,
        ],
        compiler_params=pltpu.CompilerParams(
            collective_id=1, has_side_effects=True, vmem_limit_bytes=32 * 2**20
        ),
    )(attended)


def attend_kernel(block, q_ref, k_ref, v_ref, lam_ref, gain_ref, o_ref):
    length, width = q_ref.shape
    value_size = gain_ref.shape[1]
    heads = width // value_size
    half = value_size // 2
    lane = lax.broadcasted_iota(jnp.int32, (block, value_size), 1)
    row = lax.broadcasted_iota(jnp.int32, (block, block), 0)
    col = lax.broadcasted_iota(jnp.int32, (block, block), 1)
    causal = col <= row
    contract = (((1,), (1,)), ((), ()))
    for head in range(heads):
        cols = slice(head * value_size, (head + 1) * value_size)
        for step in range(length // block):
            rows = slice(step * block, (step + 1) * block)
            past = step * block
            query = q_ref[rows, cols]
            near, far = [], []
            for which in range(2):
                keep = (lane < half) if which == 0 else (lane >= half)
                part = jnp.where(keep, query, jnp.zeros_like(query))
                s_near = lax.dot_general(
                    part, k_ref[rows, cols], contract, preferred_element_type=jnp.float32
                ) * (half**-0.5)
                s_near = jnp.where(causal, s_near, -jnp.inf)
                top = jnp.max(s_near, axis=-1, keepdims=True)
                if past:
                    s_far = lax.dot_general(
                        part, k_ref[:past, cols], contract, preferred_element_type=jnp.float32
                    ) * (half**-0.5)
                    top = jnp.maximum(top, jnp.max(s_far, axis=-1, keepdims=True))
                e_near = jnp.exp(s_near - top)
                total = jnp.sum(e_near, axis=-1, keepdims=True)
                if past:
                    e_far = jnp.exp(s_far - top)
                    total = total + jnp.sum(e_far, axis=-1, keepdims=True)
                scale = 1.0 / total
                if which == 1:
                    scale = scale * lam_ref[head]
                near.append(e_near * scale)
                if past:
                    far.append(e_far * scale)
            mixture = (near[0] - near[1]).astype(jnp.bfloat16)
            result = jnp.dot(mixture, v_ref[rows, cols], preferred_element_type=jnp.float32)
            if past:
                mixture = (far[0] - far[1]).astype(jnp.bfloat16)
                result += jnp.dot(
                    mixture, v_ref[:past, cols], preferred_element_type=jnp.float32
                )
            o_ref[rows, cols] = rms_scale(result, gain_ref[...]).astype(o_ref.dtype)


def attend(q, k, v, head_lambda, head_gain):
    return pl.pallas_call(
        functools.partial(attend_kernel, min(256, q.shape[0])),
        out_shape=jax.ShapeDtypeStruct(q.shape, q.dtype),
        in_specs=[VMEM] * 3 + [pl.BlockSpec(memory_space=pltpu.SMEM), VMEM],
        out_specs=VMEM,
        compiler_params=pltpu.CompilerParams(vmem_limit_bytes=48 * 2**20),
    )(q, k, v, head_lambda, head_gain.reshape(1, -1))


def half_place(sp_half, dp_size):
    sp, dp = lax.axis_index("sp"), lax.axis_index("dp")
    first = sp // sp_half * sp_half
    here = (sp - first) * dp_size + dp
    mirror = {"sp": lax.rem(sp + sp_half, 2 * sp_half), "dp": dp}

    def peer(place):
        return {"sp": first + place // dp_size, "dp": lax.rem(place, dp_size)}

    return here, mirror, peer


def half_barrier(group, here, mirror, peer):
    barrier = pltpu.get_barrier_semaphore()
    pl.semaphore_signal(barrier, inc=1, device_id=mirror, device_id_type=MESH)

    def greet(off, carry):
        pl.semaphore_signal(
            barrier, inc=1, device_id=peer(lax.rem(here + off, group)), device_id_type=MESH
        )
        return carry

    lax.fori_loop(1, group, greet, 0)
    pl.semaphore_wait(barrier, group)


def experts_kernel(
    sp_half,
    dp_size,
    normed_ref,
    own_pick_ref,
    far_pick_ref,
    high_ref,
    low_ref,
    gate_hbm,
    up_hbm,
    down_hbm,
    o_ref,
    far_ref,
    gate_w,
    up_w,
    down_w,
    own_rows,
    tokens,
    rows,
    own_in,
    far_in,
    flat,
    hidden,
    own_out,
    far_out,
    landed,
    partial,
    send_sem,
    recv_sem,
    back_send,
    back_recv,
    far_send,
    far_recv,
    local_sem,
):
    group = sp_half * dp_size
    chunks, _, cap, width = rows.shape
    here, mirror, peer = half_place(sp_half, dp_size)
    half_barrier(group, here, mirror, peer)

    def cols(chunk):
        return pl.ds(chunk * width, width)

    def far(way, chunk):
        return pltpu.make_async_remote_copy(
            src_ref=(partial.at[chunk] if way else normed_ref.at[:, cols(chunk)]),
            dst_ref=(far_ref.at[:, cols(chunk)] if way else tokens.at[chunk]),
            send_sem=far_send.at[way, chunk],
            recv_sem=far_recv.at[way, chunk],
            device_id=mirror,
            device_id_type=MESH,
        )

    def send(off, source, target, row, sends, recvs):
        place = lax.rem(here + off, group)
        return pltpu.make_async_remote_copy(
            src_ref=source(place),
            dst_ref=target(here),
            send_sem=sends.at[row, off],
            recv_sem=recvs.at[row, off],
            device_id=peer(place),
            device_id_type=MESH,
        )

    def keep(source, target, index):
        return pltpu.make_async_copy(source(here), target(here), local_sem.at[index])

    def over(action):
        lax.fori_loop(1, group, lambda off, carry: (action(off), carry)[1], 0)

    out_own = (lambda p: own_rows.at[p], lambda p: own_in.at[p])
    back_own = (lambda p: own_out.at[p], lambda p: o_ref.at[p])

    def out_far(chunk):
        return (lambda p: rows.at[chunk, p], lambda p: far_in.at[p, :, cols(chunk)])

    def back_far(chunk):
        return (lambda p: far_out.at[p, :, cols(chunk)], lambda p: landed.at[chunk, p])

    def near(off):
        return send(off, *out_own, chunks, send_sem, recv_sem)

    def passed(chunk, off):
        return send(off, *out_far(chunk), chunk, send_sem, recv_sem)

    def near_back(off):
        return send(off, *back_own, chunks, back_send, back_recv)

    def passed_back(chunk, off):
        return send(off, *back_far(chunk), chunk, back_send, back_recv)

    loads = [
        pltpu.make_async_copy(source, target, local_sem.at[2 * chunks + 2 + index])
        for index, (source, target) in enumerate(
            ((gate_hbm, gate_w), (up_hbm, up_w), (down_hbm, down_w))
        )
    ]
    tile = min(256, gate_w.shape[1])

    def hidden_of(block):
        for chunk in range(chunks):
            part = block[:, :, chunk * width : (chunk + 1) * width].astype(jnp.float32)
            flat[:, chunk * width : (chunk + 1) * width] = part.reshape(
                group * cap, width
            ).astype(flat.dtype)

        def one(index, carry):
            some = columns_of(index, tile)
            gate_val = jnp.dot(flat[...], gate_w[:, some], preferred_element_type=jnp.float32)
            up_val = jnp.dot(flat[...], up_w[:, some], preferred_element_type=jnp.float32)
            hidden[:, some] = (jax.nn.silu(gate_val) * up_val).astype(hidden.dtype)
            return carry

        lax.fori_loop(0, gate_w.shape[1] // tile, one, 0)

    def down_to(target, chunk):
        part = slice(chunk * width, (chunk + 1) * width)
        value = jnp.dot(hidden[...], down_w[:, part], preferred_element_type=jnp.float32)
        target[:, :, part] = value.reshape(group, cap, width).astype(target.dtype)

    for chunk in range(chunks):
        far(0, chunk).start()
    for chunk in range(chunks):
        part = slice(chunk * width, (chunk + 1) * width)
        value = jnp.dot(
            own_pick_ref[...], normed_ref[:, part], preferred_element_type=jnp.float32
        )
        own_rows[:, :, part] = value.reshape(group, cap, width).astype(own_rows.dtype)
    over(lambda off: near(off).start())
    keep(*out_own, 2 * chunks).start()
    for load in loads:
        load.start()
    for chunk in range(chunks):
        far(0, chunk).wait_recv()
        picked = jnp.dot(far_pick_ref[...], tokens[chunk], preferred_element_type=jnp.float32)
        rows[chunk] = picked.reshape(rows.shape[1:]).astype(rows.dtype)
        over(lambda off: passed(chunk, off).start())
        keep(*out_far(chunk), chunk).start()

    for load in loads:
        load.wait()
    keep(*out_own, 2 * chunks).wait()
    over(lambda off: near(off).wait_recv())
    hidden_of(own_in)
    for chunk in range(chunks):
        down_to(own_out, chunk)
    over(lambda off: near_back(off).start())
    keep(*back_own, 2 * chunks + 1).start()

    for chunk in range(chunks):
        keep(*out_far(chunk), chunk).wait()
        over(lambda off: passed(chunk, off).wait_recv())
    hidden_of(far_in)
    for chunk in range(chunks):
        down_to(far_out, chunk)
        over(lambda off: passed_back(chunk, off).start())
        keep(*back_far(chunk), chunks + chunk).start()

    contract = (((0,), (0,)), ((), ()))
    for chunk in range(chunks):
        keep(*back_far(chunk), chunks + chunk).wait()
        over(lambda off: passed_back(chunk, off).wait_recv())
        block = landed[chunk].astype(jnp.float32).reshape(group * cap, width)
        block = block.astype(jnp.bfloat16)
        total = lax.dot_general(high_ref[...], block, contract, preferred_element_type=jnp.float32)
        total += lax.dot_general(low_ref[...], block, contract, preferred_element_type=jnp.float32)
        partial[chunk] = total.astype(partial.dtype)
        far(1, chunk).start()

    keep(*back_own, 2 * chunks + 1).wait()
    over(lambda off: near(off).wait_send())
    over(lambda off: near_back(off).wait())
    for chunk in range(chunks):
        over(lambda off: passed(chunk, off).wait_send())
        over(lambda off: passed_back(chunk, off).wait_send())
        far(0, chunk).wait_send()
        far(1, chunk).wait()


def run_experts(sp_half, dp_size, cap, chunks, normed, picks, parts, gate, up, down):
    group = sp_half * dp_size
    tok, model = normed.shape
    ff = gate.shape[1]
    width = model // chunks
    kind = normed.dtype
    whole = pltpu.VMEM((group, cap, model), kind)
    pieces = pltpu.VMEM((chunks, group, cap, width), kind)
    token_pieces = pltpu.VMEM((chunks, tok, width), kind)
    return pl.pallas_call(
        functools.partial(experts_kernel, sp_half, dp_size),
        out_shape=[
            jax.ShapeDtypeStruct((group, cap, model), kind),
            jax.ShapeDtypeStruct((tok, model), kind),
        ],
        in_specs=[VMEM] * 5 + [pl.BlockSpec(memory_space=pl.ANY)] * 3,
        out_specs=[VMEM] * 2,
        scratch_shapes=[
            pltpu.VMEM((model, ff), kind),
            pltpu.VMEM((model, ff), kind),
            pltpu.VMEM((ff, model), kind),
            whole,
            token_pieces,
            pieces,
            whole,
            whole,
            pltpu.VMEM((group * cap, model), kind),
            pltpu.VMEM((group * cap, ff), kind),
            whole,
            whole,
            pieces,
            token_pieces,
        ]
        + [pltpu.SemaphoreType.DMA((chunks + 1, group))] * 4
        + [pltpu.SemaphoreType.DMA((2, chunks))] * 2
        + [pltpu.SemaphoreType.DMA((2 * chunks + 5,))],
        compiler_params=pltpu.CompilerParams(
            collective_id=2, has_side_effects=True, vmem_limit_bytes=56 * 2**20
        ),
    )(normed, *picks, *parts, gate, up, down)


def slot_tables(chosen, weights, first, group, cap):
    tok = chosen.shape[0]
    ids = first + jnp.arange(group, dtype=jnp.int32)
    named = chosen.T[None] == ids[:, None, None]
    member = jnp.sum(named.astype(jnp.float32), axis=1)
    weight = jnp.sum(jnp.where(named, weights.T[None], 0.0), axis=1)
    before = jnp.arange(tok)[:, None] < jnp.arange(tok)[None, :]
    earlier = jnp.dot(
        member.astype(jnp.bfloat16),
        before.astype(jnp.bfloat16),
        preferred_element_type=jnp.float32,
    )
    rank = jnp.where(member > 0, earlier, -1.0)
    hit = rank[:, None, :] == jnp.arange(cap, dtype=jnp.float32)[None, :, None]
    spread = jnp.where(hit, weight[:, None, :], 0.0)
    high = spread.astype(jnp.bfloat16)
    low = (spread - high.astype(jnp.float32)).astype(jnp.bfloat16)
    flat = (group * cap, tok)
    return hit.astype(jnp.bfloat16).reshape(flat), high.reshape(flat), low.reshape(flat)


def local(
    queries,
    key_vectors,
    value_vectors,
    head_lambda,
    head_gain,
    residual,
    out_weight,
    mix_gain,
    pre_gain,
    post_gain,
    routes,
    route_weights,
    expert_gate,
    expert_up,
    expert_down,
    shared_gate,
    shared_up,
    shared_down,
):
    n, dp_size = lax.axis_size("sp"), lax.axis_size("dp")
    sp_half = n // 2
    group = sp_half * dp_size
    tok = queries.shape[1]
    top_count = routes.shape[2]
    cap = 3 * tok * top_count // (2 * n * dp_size)
    cap = (cap + 7) // 8 * 8
    model = residual.shape[2]
    chunks = 4

    sent = jnp.concatenate([routes[0].astype(jnp.float32), route_weights[0]], axis=1)
    sent = jnp.pad(sent, ((0, 0), (0, 128 - 2 * top_count)))

    q, k, v, far_sent = to_heads(
        n,
        queries.reshape(tok, -1),
        key_vectors.reshape(tok, -1),
        value_vectors.reshape(tok, -1),
        sent,
    )
    width = q.shape[2]
    attended = attend(
        q.reshape(-1, width), k.reshape(-1, width), v.reshape(-1, width), head_lambda, head_gain
    )
    flat_heads = to_tokens(n, attended.reshape(n, tok, width))

    first = lax.axis_index("sp") // sp_half * group
    pick, high, low = slot_tables(routes[0], route_weights[0], first, group, cap)
    far_pick, far_high, far_low = slot_tables(
        far_sent[:, :top_count].astype(jnp.int32), far_sent[:, top_count : 2 * top_count], first, group, cap
    )

    mixed_rows = jnp.dot(flat_heads, out_weight, preferred_element_type=jnp.float32)
    updated = (residual[0].astype(jnp.float32) + rms_scale(mixed_rows, mix_gain)).astype(
        jnp.bfloat16
    )
    normed = rms_scale(updated.astype(jnp.float32), pre_gain).astype(jnp.bfloat16)
    returned, from_far = run_experts(
        sp_half,
        dp_size,
        cap,
        chunks,
        normed,
        (pick, far_pick),
        (far_high, far_low),
        expert_gate[0],
        expert_up[0],
        expert_down[0],
    )
    shared_out = feed_forward(normed, shared_gate, shared_up, shared_down)
    rows = returned.reshape(group * cap, model)
    contract = (((0,), (0,)), ((), ()))
    routed = lax.dot_general(high, rows, contract, preferred_element_type=jnp.float32)
    routed += lax.dot_general(low, rows, contract, preferred_element_type=jnp.float32)
    combined = routed + from_far.astype(jnp.float32) + shared_out.astype(jnp.float32)
    output = (updated.astype(jnp.float32) + rms_scale(combined, post_gain)).astype(jnp.bfloat16)
    return output.reshape(1, tok, model)


def solution(mesh):
    in_specs = (
        P("dp", "sp", None, None),
        P("dp", "sp", None, None),
        P("dp", "sp", None, None),
        P("sp"),
        P(),
        P("dp", "sp", None),
        P(),
        P(),
        P(),
        P(),
        P("dp", "sp", None),
        P("dp", "sp", None),
        P(("sp", "dp"), None, None),
        P(("sp", "dp"), None, None),
        P(("sp", "dp"), None, None),
        P(),
        P(),
        P(),
    )
    out_specs = P("dp", "sp", None)
    return jax.shard_map(local, mesh=mesh, in_specs=in_specs, out_specs=out_specs, check_vma=False)
```

profile of v0, /device:TPU:0, one launch (start us, length us, event | category | flops | bytes accessed | tf_op | source)
XLA Modules:
  0.0 195.3 jit_solution(17538207726483506085)
XLA Ops:
  0.0 0.8 bitcast_convert_fusion
  0.8 0.7 pad_maximum_fusion
  1.5 0.1 eq.78
  1.6 0.1 copy.28
  1.7 1.2 copy.37
  2.9 0.0 copy-start.1
  2.9 0.0 copy-start.2
  2.9 1.4 copy_bitcast_fusion
  4.4 44.1 %shard_map.172 = (bf16[8,128,256]{2,1,0:T(8,128)(2,1)S(1)}, bf16[8,128,256]{2,1,0:T(8,128)(2,1)S(1)}, bf16[8,128,256]{2,1,0:T(8,128)(2,1)S(1)}, f32[128,128]{1,0:T(8,128)S(1)}) custom-call(bf16[128,2048]{1,0:T(8,128)(2,1)S(1)} %bitcast.81, bf16[128,2048]{1,0:T(8,128)(2,1)S(1)} %get-tuple-element.34.k_ref, bf16[128,2048]{1,0:T(8,128)(2,1)S(1)} %get-tuple-element.33.v_ref, ...), custom_call_target="tpu_custom_call" | custom-call | tf_op jit(solution)/shard_map/pallas_call | solution.py:118
  48.6 5.9 %shard_map.173 = bf16[1024,256]{1,0:T(8,128)(2,1)S(1)} custom-call(bf16[1024,256]{1,0:T(8,128)(2,1)S(1)} %bitcast.83, bf16[1024,256]{1,0:T(8,128)(2,1)S(1)} %bitcast.84, bf16[1024,256]{1,0:T(8,128)(2,1)S(1)} %bitcast.85, f32[2]{0:T(128)S(1)} %copy-done.1, f32[1,128]{1,0:T(1,128)S(1)} %bitcast.86), custom_call_target="tpu_custom_call" | custom-call | tf_op jit(solution)/shard_map/pallas_call | solution.py:237
  54.5 12.6 %shard_map.174 = bf16[128,2048]{1,0:T(8,128)(2,1)S(1)} custom-call(bf16[8,128,256]{2,1,0:T(8,128)(2,1)S(1)} %bitcast.82), custom_call_target="tpu_custom_call" | custom-call | tf_op jit(solution)/shard_map/pallas_call | solution.py:169
  67.1 0.1 slice_bitcast_fusion
  67.2 0.1 copy.30
  67.3 0.1 copy.29
  67.3 0.1 fusion.31
  67.5 0.1 convolution_select_fusion.1
  67.6 0.1 convolution_select_fusion
  67.7 0.8 fusion.19.low_ref
  68.5 0.7 fusion.18.high_ref
  69.2 0.8 fusion.20
  70.0 4.8 %multiply_reduce_fusion.1 = (f32[128]{0:T(128)S(1)}, f32[128,2048]{1,0:T(8,128)S(1)}) fusion(bf16[128,2048]{1,0:T(8,128)(2,1)S(1)} %shard_map.174, bf16[2048,2048]{1,0:T(8,128)(2,1)} %param.24), kind=kOutput, calls=%fused_computation.21 | convolution fusion | flops 1074265984 | bytes 9961984 | tf_op jit(solution)/shard_map/dot_general | solution.py:566
  74.9 0.4 fusion.5
  75.3 0.3 copy-done.9
  75.5 0.2 fusion.7.normed_ref
  75.7 0.7 copy-done.6
  76.4 0.4 fusion.40
  76.9 3.4 %fusion.3 = f32[128,2048]{1,0:T(8,128)} fusion(bf16[512,2048]{1,0:T(8,128)(2,1)S(1)} %copy-done, bf16[128,2048]{1,0:T(8,128)(2,1)S(1)} %fusion.7.normed_ref, bf16[2048,512]{1,0:T(8,128)(2,1)} %param.34, f32[128,512]{1,0:T(8,128)S(1)} %fusion.40), kind=kOutput, calls=%fused_computation.6 | convolution fusion | flops 537788416 | bytes 6029312 | tf_op jit(solution)/shard_map/dot_general | solution.py:27
  80.3 110.1 %shard_map.175 = (bf16[16,24,2048]{2,1,0:T(8,128)(2,1)}, bf16[128,2048]{1,0:T(8,128)(2,1)}) custom-call(bf16[128,2048]{1,0:T(8,128)(2,1)} %copy-done.3, bf16[384,128]{1,0:T(8,128)(2,1)} %get-tuple-element.28.own_pick_ref, bf16[384,128]{1,0:T(8,128)(2,1)} %get-tuple-element.27.far_pick_ref, bf16[384,128]{1,0:T(8,128)(2,1)} %fusion.18.high_ref, ...), custom_call_target="tpu_custom_call" | custom-call | tf_op jit(solution)/shard_map/pallas_call | solution.py:460
  190.4 2.0 %convolution_bitcast_fusion = f32[128,2048]{1,0:T(8,128)S(1)} fusion(bf16[16,24,2048]{2,1,0:T(8,128)(2,1)} %get-tuple-element.15, f32[16,128]{1,0:T(8,128)S(1)} %get-tuple-element.17, f32[16,128]{1,0:T(8,128)S(1)} %convolution_select_fusion.1), kind=kOutput, calls=%fused_computation | convolution fusion | flops 201621504 | bytes 2637824 | tf_op jit(solution)/shard_map/dot_general | solution.py:587
  192.4 0.1 copy-done.5
  192.5 1.7 multiply_reduce_fusion
  194.2 1.0 fusion.10
  (27 shorter events, 0.1 us)
Async XLA Ops:
  0.0 76.9 %copy-start = (bf16[512,2048]{1,0:T(8,128)(2,1)S(1)}, bf16[512,2048]{1,0:T(8,128)(2,1)}, u32[]{:S(2)}) copy-start(bf16[512,2048]{1,0:T(8,128)(2,1)} %param.35) | copy-start | bytes 6291460
  2.9 45.6 %copy-start.1 = (f32[2]{0:T(128)S(1)}, f32[2]{0:T(128)}, u32[]{:S(2)}) copy-start(f32[2]{0:T(128)} %lam_ref.1) | copy-start | bytes 28
  2.9 45.6 %copy-start.2 = (f32[128]{0:T(128)S(1)}, f32[128]{0:T(128)}, u32[]{:S(2)}) copy-start(f32[128]{0:T(128)} %param.22) | copy-start | bytes 1540
  48.5 18.8 %copy-start.11 = (s32[1,128,4]{1,2,0:T(4,128)S(1)}, s32[1,128,4]{1,2,0:T(4,128)}, u32[]{:S(2)}) copy-start(s32[1,128,4]{1,2,0:T(4,128)} %param.28) | copy-start | bytes 6148
  48.5 18.8 %copy-start.12 = (f32[1,128,4]{1,2,0:T(4,128)S(1)}, f32[1,128,4]{1,2,0:T(4,128)}, u32[]{:S(2)}) copy-start(f32[1,128,4]{1,2,0:T(4,128)} %param.29) | copy-start | bytes 6148
  70.0 4.8 %copy-start.7 = (bf16[1,128,2048]{2,1,0:T(8,128)(2,1)S(1)}, bf16[1,128,2048]{2,1,0:T(8,128)(2,1)}, u32[]{:S(2)}) copy-start(bf16[1,128,2048]{2,1,0:T(8,128)(2,1)} %param.23) | copy-start | bytes 1572868
  70.0 4.8 %copy-start.8 = (f32[2048]{0:T(1024)S(1)}, f32[2048]{0:T(1024)}, u32[]{:S(2)}) copy-start(f32[2048]{0:T(1024)} %param.25) | copy-start | bytes 24580
  74.8 0.7 copy-start.9
  74.8 1.6 copy-start.6
  76.4 3.9 %copy-start.3 = (bf16[128,2048]{1,0:T(8,128)(2,1)}, bf16[128,2048]{1,0:T(8,128)(2,1)S(1)}, u32[]{:S(2)}) copy-start(bf16[128,2048]{1,0:T(8,128)(2,1)S(1)} %fusion.7.normed_ref) | copy-start | bytes 1572868
  190.4 2.1 %copy-start.4 = (bf16[16,24,2048]{2,1,0:T(8,128)(2,1)S(1)}, bf16[16,24,2048]{2,1,0:T(8,128)(2,1)}, u32[]{:S(2)}) copy-start(bf16[16,24,2048]{2,1,0:T(8,128)(2,1)} %get-tuple-element.15) | copy-start | bytes 4718596
  190.4 2.2 %copy-start.5 = (f32[128,2048]{1,0:T(8,128)S(1)}, f32[128,2048]{1,0:T(8,128)}, u32[]{:S(2)}) copy-start(f32[128,2048]{1,0:T(8,128)} %fusion.3) | copy-start | bytes 3145732
  192.5 1.7 copy-start.10
where the time goes:
time: 199 us; the launch traced here: 195 us
  Pallas kernels  173 us (87%)
  matrix products  12.6 us (6%)
  other arithmetic  5.63 us (3%)
  local copies, waits for them, and re-layouts  4.11 us (2%)
    pallas_call x1, Pallas kernels, run_experts(): pl.pallas_call(functools.partial(experts_kernel, sp_half, dp_size), out_s...  110 us
    pallas_call x1, Pallas kernels, to_heads(): pl.pallas_call(functools.partial(to_heads_kernel, n), out_shape=[out] * 3...  44.1 us
    pallas_call x1, Pallas kernels, to_tokens(): pl.pallas_call(functools.partial(to_tokens_kernel, n), out_shape=jax.Shap...  12.6 us
    pallas_call x1, Pallas kernels, attend(): pl.pallas_call(functools.partial(attend_kernel, min(256, q.shape[0])), ou...  5.9 us
    dot_general x1, matrix products, local(): jnp.dot(flat_heads, out_weight, preferred_element_type=jnp.float32)  4.78 us

commit v1 on v0

v1 whole, which is shorter than its diff:
```python
import functools

import jax
import jax.numpy as jnp
from jax import lax
from jax.experimental import pallas as pl
from jax.experimental.pallas import tpu as pltpu
from jax.sharding import PartitionSpec as P

epsilon = 1e-06
MESH = pl.DeviceIdType.MESH
VMEM = pl.BlockSpec(memory_space=pltpu.VMEM)


def rms_scale(values_in, gain):
    return (
        values_in
        * lax.rsqrt(jnp.mean(values_in * values_in, axis=-1, keepdims=True) + epsilon)
        * gain
    )


def columns_of(index, width):
    return pl.ds(pl.multiple_of(index * width, width), width)


def line_barrier(n, me):
    barrier = pltpu.get_barrier_semaphore()

    def greet(off, carry):
        pl.semaphore_signal(
            barrier, inc=1, device_id={"sp": lax.rem(me + off, n)}, device_id_type=MESH
        )
        return carry

    lax.fori_loop(1, n, greet, 0)
    pl.semaphore_wait(barrier, n - 1)


def to_heads_kernel(
    n,
    q_ref,
    k_ref,
    v_ref,
    qo_ref,
    ko_ref,
    vo_ref,
    send_sem,
    recv_sem,
    own_sem,
):
    me = lax.axis_index("sp")
    width = qo_ref.shape[2]
    pairs = ((q_ref, qo_ref), (k_ref, ko_ref), (v_ref, vo_ref))
    line_barrier(n, me)

    def copy(which, off):
        source, target = pairs[which]
        dst = lax.rem(me + off, n)
        return pltpu.make_async_remote_copy(
            src_ref=source.at[:, columns_of(dst, width)],
            dst_ref=target.at[me],
            send_sem=send_sem.at[which, off],
            recv_sem=recv_sem.at[which, off],
            device_id={"sp": dst},
            device_id_type=MESH,
        )

    def own(which):
        source, target = pairs[which]
        return pltpu.make_async_copy(
            source.at[:, columns_of(me, width)], target.at[me], own_sem.at[which]
        )

    def start(off, carry):
        for which in range(3):
            copy(which, off).start()
        return carry

    def finish(off, carry):
        for which in range(3):
            copy(which, off).wait()
        return carry

    lax.fori_loop(1, n, start, 0)
    for which in range(3):
        own(which).start()
    for which in range(3):
        own(which).wait()
    lax.fori_loop(1, n, finish, 0)


def to_heads(n, q, k, v):
    tok, model = q.shape
    width = model // n
    out = jax.ShapeDtypeStruct((n, tok, width), q.dtype)
    return pl.pallas_call(
        functools.partial(to_heads_kernel, n),
        out_shape=[out] * 3,
        in_specs=[VMEM] * 3,
        out_specs=[VMEM] * 3,
        scratch_shapes=[
            pltpu.SemaphoreType.DMA((3, n)),
            pltpu.SemaphoreType.DMA((3, n)),
            pltpu.SemaphoreType.DMA((3,)),
        ],
        compiler_params=pltpu.CompilerParams(
            collective_id=0, has_side_effects=True, vmem_limit_bytes=32 * 2**20
        ),
    )(q, k, v)


def to_tokens_kernel(n, a_ref, o_ref, send_sem, recv_sem, own_sem):
    me = lax.axis_index("sp")
    width = a_ref.shape[2]
    line_barrier(n, me)

    def copy(off):
        dst = lax.rem(me + off, n)
        return pltpu.make_async_remote_copy(
            src_ref=a_ref.at[dst],
            dst_ref=o_ref.at[:, columns_of(me, width)],
            send_sem=send_sem.at[off],
            recv_sem=recv_sem.at[off],
            device_id={"sp": dst},
            device_id_type=MESH,
        )

    def start(off, carry):
        copy(off).start()
        return carry

    def finish(off, carry):
        copy(off).wait()
        return carry

    lax.fori_loop(1, n, start, 0)
    own = pltpu.make_async_copy(a_ref.at[me], o_ref.at[:, columns_of(me, width)], own_sem)
    own.start()
    own.wait()
    lax.fori_loop(1, n, finish, 0)


def to_tokens(n, attended):
    _, tok, width = attended.shape
    return pl.pallas_call(
        functools.partial(to_tokens_kernel, n),
        out_shape=jax.ShapeDtypeStruct((tok, n * width), attended.dtype),
        in_specs=[VMEM],
        out_specs=VMEM,
        scratch_shapes=[
            pltpu.SemaphoreType.DMA((n,)),
            pltpu.SemaphoreType.DMA((n,)),
            pltpu.SemaphoreType.DMA,
        ],
        compiler_params=pltpu.CompilerParams(
            collective_id=1, has_side_effects=True, vmem_limit_bytes=32 * 2**20
        ),
    )(attended)


def attend_kernel(block, q_ref, k_ref, v_ref, lam_ref, gain_ref, o_ref):
    length, width = q_ref.shape
    value_size = gain_ref.shape[1]
    heads = width // value_size
    half = value_size // 2
    lane = lax.broadcasted_iota(jnp.int32, (block, value_size), 1)
    row = lax.broadcasted_iota(jnp.int32, (block, block), 0)
    col = lax.broadcasted_iota(jnp.int32, (block, block), 1)
    causal = col <= row
    contract = (((1,), (1,)), ((), ()))
    for head in range(heads):
        cols = slice(head * value_size, (head + 1) * value_size)
        for step in range(length // block):
            rows = slice(step * block, (step + 1) * block)
            past = step * block
            query = q_ref[rows, cols]
            near, far = [], []
            for which in range(2):
                keep = (lane < half) if which == 0 else (lane >= half)
                part = jnp.where(keep, query, jnp.zeros_like(query))
                s_near = lax.dot_general(
                    part, k_ref[rows, cols], contract, preferred_element_type=jnp.float32
                ) * (half**-0.5)
                s_near = jnp.where(causal, s_near, -jnp.inf)
                top = jnp.max(s_near, axis=-1, keepdims=True)
                if past:
                    s_far = lax.dot_general(
                        part, k_ref[:past, cols], contract, preferred_element_type=jnp.float32
                    ) * (half**-0.5)
                    top = jnp.maximum(top, jnp.max(s_far, axis=-1, keepdims=True))
                e_near = jnp.exp(s_near - top)
                total = jnp.sum(e_near, axis=-1, keepdims=True)
                if past:
                    e_far = jnp.exp(s_far - top)
                    total = total + jnp.sum(e_far, axis=-1, keepdims=True)
                scale = 1.0 / total
                if which == 1:
                    scale = scale * lam_ref[head]
                near.append(e_near * scale)
                if past:
                    far.append(e_far * scale)
            mixture = (near[0] - near[1]).astype(jnp.bfloat16)
            result = jnp.dot(mixture, v_ref[rows, cols], preferred_element_type=jnp.float32)
            if past:
                mixture = (far[0] - far[1]).astype(jnp.bfloat16)
                result += jnp.dot(
                    mixture, v_ref[:past, cols], preferred_element_type=jnp.float32
                )
            o_ref[rows, cols] = rms_scale(result, gain_ref[...]).astype(o_ref.dtype)


def attend(q, k, v, head_lambda, head_gain):
    return pl.pallas_call(
        functools.partial(attend_kernel, min(256, q.shape[0])),
        out_shape=jax.ShapeDtypeStruct(q.shape, q.dtype),
        in_specs=[VMEM] * 3 + [pl.BlockSpec(memory_space=pltpu.SMEM), VMEM],
        out_specs=VMEM,
        compiler_params=pltpu.CompilerParams(vmem_limit_bytes=48 * 2**20),
    )(q, k, v, head_lambda, head_gain.reshape(1, -1))


def drain(ref, sem):
    pltpu.make_async_copy(ref, ref, sem).wait()


def experts_kernel(
    planes,
    inner,
    dp_size,
    chunks,
    top,
    normed_ref,
    updated_ref,
    side_ref,
    gain_ref,
    gate_hbm,
    up_hbm,
    down_hbm,
    sgate_hbm,
    sup_hbm,
    sdown_hbm,
    o_ref,
    gate_w,
    up_w,
    down_w,
    sgate_w,
    sup_w,
    sdown_w,
    sides,
    tokens,
    slots_a,
    slots_b,
    pick,
    high,
    low,
    rows,
    inbox,
    flat,
    hidden,
    outs,
    landed,
    partial,
    sums,
    total,
    load_sem,
    side_send,
    side_recv,
    z_send,
    z_recv,
    out_send,
    out_recv,
    back_send,
    back_recv,
    sum_send,
    sum_recv,
):
    group = inner * dp_size
    _, _, _, cap, width = rows.shape
    tok = normed_ref.shape[0]
    cores = 2 if dp_size % 2 == 0 else 1
    chips = dp_size // cores
    sp, dp = lax.axis_index("sp"), lax.axis_index("dp")
    z, y = sp // inner, lax.rem(sp, inner)
    place = y * dp_size + dp
    last = planes - 1
    has_up, has_down = z < last, z > 0
    is_end = lax.rem(z, last) == 0

    def peer(k):
        core = lax.rem(lax.rem(dp, cores) + lax.rem(k, cores), cores)
        chip = lax.rem(dp // cores + lax.rem(k // cores, chips), chips)
        row = lax.rem(y + k // dp_size, inner)
        there = chip * cores + core
        return row * dp_size + there, {"sp": z * inner + row, "dp": there}

    def column(plane):
        return {"sp": plane * inner + y, "dp": dp}

    def over(first, stop, action):
        lax.fori_loop(first, stop, lambda i, carry: (action(i), carry)[1], 0)

    barrier = pltpu.get_barrier_semaphore()
    over(
        1,
        group,
        lambda k: pl.semaphore_signal(
            barrier, inc=1, device_id=peer(k)[1], device_id_type=MESH
        ),
    )
    for d in range(1, planes):
        pl.semaphore_signal(
            barrier, inc=1, device_id=column(lax.rem(z + d, planes)), device_id_type=MESH
        )
    pl.semaphore_wait(barrier, group - 1 + planes - 1)

    loads = [
        pltpu.make_async_copy(source, target, load_sem.at[index])
        for index, (source, target) in enumerate(
            (
                (sgate_hbm, sgate_w),
                (sup_hbm, sup_w),
                (sdown_hbm, sdown_w),
                (gate_hbm, gate_w),
                (up_hbm, up_w),
                (down_hbm, down_w),
            )
        )
    ]

    def side(d):
        return pltpu.make_async_remote_copy(
            src_ref=side_ref,
            dst_ref=sides.at[z],
            send_sem=side_send.at[d],
            recv_sem=side_recv.at[z],
            device_id=column(lax.rem(z + d, planes)),
            device_id_type=MESH,
        )

    def push(block, chunk, up):
        return pltpu.make_async_remote_copy(
            src_ref=tokens.at[block, chunk],
            dst_ref=tokens.at[block, chunk],
            send_sem=z_send.at[up, block, chunk],
            recv_sem=z_recv.at[block, chunk],
            device_id=column(z + 2 * up - 1),
            device_id_type=MESH,
        )

    def pushes(block, own, action):
        @pl.when(jnp.logical_and(has_up, True if own else block < z))
        def _():
            action(1)

        @pl.when(jnp.logical_and(has_down, True if own else block > z))
        def _():
            action(0)

    def block_of(slot):
        if slot == 0:
            return z
        if slot == 1:
            return 1 + lax.rem(z, 2)
        if slot == 2:
            return lax.rem(2 + 3 * z, 5)
        return 3 * (1 - z // 2)

    def deal(slot, chunk):
        def one(k):
            there, device = peer(k)
            pltpu.make_async_remote_copy(
                src_ref=rows.at[slot, chunk, there],
                dst_ref=inbox.at[slot, chunk, place],
                send_sem=out_send.at[slot, chunk],
                recv_sem=out_recv.at[slot, chunk],
                device_id=device,
                device_id_type=MESH,
            ).start()

        over(1, group, one)

    def give_back(slot, chunk):
        def one(k):
            there, device = peer(k)
            pltpu.make_async_remote_copy(
                src_ref=outs.at[slot, chunk, there],
                dst_ref=landed.at[slot, chunk, place],
                send_sem=back_send.at[slot, chunk],
                recv_sem=back_recv.at[slot, chunk],
                device_id=device,
                device_id_type=MESH,
            ).start()

        over(1, group, one)

    def others(ref, slot, chunk):
        return ref.at[slot, chunk, pl.ds(0, group - 1)]

    def tables(slot, source):
        ids = (z * group).astype(jnp.float32) + lax.broadcasted_iota(
            jnp.int32, (group, tok), 0
        ).astype(jnp.float32)
        member = jnp.zeros((group, tok), jnp.float32)
        weight = jnp.zeros((group, tok), jnp.float32)
        for j in range(top):
            named = source[j : j + 1, :] == ids
            member += jnp.where(named, 1.0, 0.0)
            weight += jnp.where(named, source[top + j : top + j + 1, :], 0.0)
        before = lax.broadcasted_iota(jnp.int32, (tok, tok), 0) < lax.broadcasted_iota(
            jnp.int32, (tok, tok), 1
        )
        earlier = jnp.dot(
            member.astype(jnp.bfloat16),
            jnp.where(before, 1.0, 0.0).astype(jnp.bfloat16),
            preferred_element_type=jnp.float32,
        )
        rank = jnp.where(member > 0, earlier, -1.0)
        seat = lax.broadcasted_iota(jnp.int32, (cap, tok), 0).astype(jnp.float32)
        for e in range(group):
            hit = rank[e : e + 1, :] == seat
            slots_a[e * cap : (e + 1) * cap, :] = jnp.where(hit, 1.0, 0.0)
            slots_b[e * cap : (e + 1) * cap, :] = jnp.where(hit, weight[e : e + 1, :], 0.0)
        pick[slot] = slots_a[...].astype(pick.dtype)
        spread = slots_b[...]
        upper = spread.astype(high.dtype)
        high[slot] = upper
        low[slot] = (spread - upper.astype(jnp.float32)).astype(low.dtype)

    def pick_rows(slot, block, chunk):
        value = jnp.dot(pick[slot], tokens[block, chunk], preferred_element_type=jnp.float32)
        rows[slot, chunk] = value.reshape(group, cap, width).astype(rows.dtype)
        inbox[slot, chunk, place] = rows[slot, chunk, place]
        deal(slot, chunk)

    def collect(slot):
        block = block_of(slot)

        def one(chunk):
            drain(tokens.at[block, chunk], z_recv.at[block, chunk])
            pushes(block, False, lambda up: push(block, chunk, up).start())
            pick_rows(slot, block, chunk)

        over(0, chunks, one)

    tile = min(256, gate_w.shape[1])
    tiles = gate_w.shape[1] // tile

    def hidden_of(source, gates, ups, target):
        def one(index, carry):
            some = columns_of(index, tile)
            gate_val = jnp.dot(source[...], gates[:, some], preferred_element_type=jnp.float32)
            up_val = jnp.dot(source[...], ups[:, some], preferred_element_type=jnp.float32)
            target[:, some] = (jax.nn.silu(gate_val) * up_val).astype(target.dtype)
            return carry

        lax.fori_loop(0, tiles, one, 0)

    def expert(slot, send):
        for chunk in range(chunks):
            drain(others(inbox, slot, chunk), out_recv.at[slot, chunk])
            part = inbox[slot, chunk].astype(jnp.float32).reshape(group * cap, width)
            flat[:, chunk * width : (chunk + 1) * width] = part.astype(flat.dtype)
        hidden_of(flat, gate_w, up_w, hidden)

        def one(chunk):
            value = jnp.dot(
                hidden[...],
                down_w[:, columns_of(chunk, width)],
                preferred_element_type=jnp.float32,
            )
            outs[slot, chunk] = value.reshape(group, cap, width).astype(outs.dtype)
            landed[slot, chunk, place] = outs[slot, chunk, place]
            if send:
                give_back(slot, chunk)

        over(0, chunks, one)

    contract = (((0,), (0,)), ((), ()))

    def combine(slot, chunk):
        drain(others(landed, slot, chunk), back_recv.at[slot, chunk])
        block = landed[slot, chunk].astype(jnp.float32).reshape(group * cap, width)
        block = block.astype(jnp.bfloat16)
        value = lax.dot_general(high[slot], block, contract, preferred_element_type=jnp.float32)
        return value + lax.dot_general(
            low[slot], block, contract, preferred_element_type=jnp.float32
        )

    def pass_sum(slot, block, chunk, up):
        target = block if up else jnp.where(z - 1 == block, planes, block)
        return pltpu.make_async_remote_copy(
            src_ref=partial.at[slot, chunk],
            dst_ref=sums.at[target, chunk],
            send_sem=sum_send.at[slot, chunk],
            recv_sem=sum_recv.at[target, chunk],
            device_id=column(z + 2 * up - 1),
            device_id_type=MESH,
        )

    def reduce_one(slot, block, chunk):
        value = combine(slot, chunk)

        @pl.when(is_end)
        def _():
            partial[slot, chunk] = value.astype(partial.dtype)

        @pl.when(jnp.logical_not(is_end))
        def _():
            drain(sums.at[block, chunk], sum_recv.at[block, chunk])
            partial[slot, chunk] = (
                value + sums[block, chunk].astype(jnp.float32)
            ).astype(partial.dtype)

        @pl.when(block > z)
        def _():
            pass_sum(slot, block, chunk, 1).start()

        @pl.when(block < z)
        def _():
            pass_sum(slot, block, chunk, 0).start()

    def reduce_all(slot):
        over(0, chunks, lambda chunk: reduce_one(slot, block_of(slot), chunk))

    for chunk in range(chunks):
        tokens[z, chunk] = normed_ref[:, chunk * width : (chunk + 1) * width]
    for d in range(1, planes):
        side(d).start()
    over(0, chunks, lambda chunk: pushes(z, True, lambda up: push(z, chunk, up).start()))
    for load in loads:
        load.start()
    tables(0, side_ref[...])
    over(0, chunks, lambda chunk: pick_rows(0, z, chunk))

    for load in loads[:3]:
        load.wait()
    shared = hidden.at[pl.ds(0, tok)]
    hidden_of(normed_ref, sgate_w, sup_w, shared)

    def shared_down(chunk):
        value = jnp.dot(
            shared[...], sdown_w[:, columns_of(chunk, width)], preferred_element_type=jnp.float32
        )
        total[chunk] = value.astype(jnp.bfloat16).astype(jnp.float32)

    over(0, chunks, shared_down)
    for slot in range(1, planes):
        block = block_of(slot)
        drain(sides.at[block], side_recv.at[block])
        tables(slot, sides[block])
    collect(1)
    for load in loads[3:]:
        load.wait()
    expert(0, False)
    collect(2)
    expert(1, True)
    collect(3)
    expert(2, True)

    @pl.when(is_end)
    def _():
        reduce_all(1)

    expert(3, True)
    over(0, chunks, lambda chunk: give_back(0, chunk))

    @pl.when(is_end)
    def _():
        reduce_all(2)
        reduce_all(3)

    @pl.when(jnp.logical_not(is_end))
    def _():
        reduce_all(1)

        def one(chunk):
            reduce_one(3, block_of(3), chunk)
            reduce_one(2, block_of(2), chunk)

        over(0, chunks, one)

    def settle(chunk):
        total[chunk] += combine(0, chunk)

        @pl.when(has_down)
        def _():
            drain(sums.at[z, chunk], sum_recv.at[z, chunk])
            total[chunk] += sums[z, chunk].astype(jnp.float32)

        @pl.when(has_up)
        def _():
            drain(sums.at[planes, chunk], sum_recv.at[planes, chunk])
            total[chunk] += sums[planes, chunk].astype(jnp.float32)

    over(0, chunks, settle)
    square = jnp.zeros((tok, 1), jnp.float32)
    for chunk in range(chunks):
        value = total[chunk]
        square += jnp.sum(value * value, axis=-1, keepdims=True)
    scale = lax.rsqrt(square / (chunks * width) + epsilon)
    for chunk in range(chunks):
        some = slice(chunk * width, (chunk + 1) * width)
        o_ref[:, some] = (
            updated_ref[:, some].astype(jnp.float32) + total[chunk] * scale * gain_ref[:, some]
        ).astype(o_ref.dtype)

    for d in range(1, planes):
        side(d).wait_send()

    def sent(chunk):
        for slot in range(planes):
            block = block_of(slot)
            pushes(block, slot == 0, lambda up: push(block, chunk, up).wait_send())
            drain(others(rows, slot, chunk), out_send.at[slot, chunk])
            drain(others(outs, slot, chunk), back_send.at[slot, chunk])
            if slot:
                drain(partial.at[slot, chunk], sum_send.at[slot, chunk])

    over(0, chunks, sent)


def run_experts(planes, inner, dp_size, cap, chunks, normed, updated, side, gain, weights):
    group = inner * dp_size
    tok, model = normed.shape
    ff = weights[0].shape[1]
    width = model // chunks
    kind = normed.dtype
    blocks = pltpu.VMEM((planes, chunks, group, cap, width), kind)
    columns = pltpu.VMEM((planes, chunks, tok, width), kind)
    table = pltpu.VMEM((planes, group * cap, tok), kind)
    wide, tall = pltpu.VMEM((model, ff), kind), pltpu.VMEM((ff, model), kind)
    dma = pltpu.SemaphoreType.DMA
    return pl.pallas_call(
        functools.partial(
            experts_kernel, planes, inner, dp_size, chunks, side.shape[0] // 2
        ),
        out_shape=jax.ShapeDtypeStruct((tok, model), kind),
        in_specs=[VMEM] * 4 + [pl.BlockSpec(memory_space=pl.ANY)] * 6,
        out_specs=VMEM,
        scratch_shapes=[
            wide,
            wide,
            tall,
            wide,
            wide,
            tall,
            pltpu.VMEM((planes,) + side.shape, side.dtype),
            columns,
            pltpu.VMEM((group * cap, tok), jnp.float32),
            pltpu.VMEM((group * cap, tok), jnp.float32),
            table,
            table,
            table,
            blocks,
            blocks,
            pltpu.VMEM((group * cap, model), kind),
            pltpu.VMEM((max(group * cap, tok), ff), kind),
            blocks,
            blocks,
            columns,
            pltpu.VMEM((planes + 1, chunks, tok, width), kind),
            pltpu.VMEM((chunks, tok, width), jnp.float32),
            dma((6,)),
            dma((planes,)),
            dma((planes,)),
            dma((2, planes, chunks)),
            dma((planes, chunks)),
            dma((planes, chunks)),
            dma((planes, chunks)),
            dma((planes, chunks)),
            dma((planes, chunks)),
            dma((planes, chunks)),
            dma((planes + 1, chunks)),
        ],
        compiler_params=pltpu.CompilerParams(
            collective_id=2, has_side_effects=True, vmem_limit_bytes=56 * 2**20
        ),
    )(normed, updated, side, gain, *weights)


def local(
    queries,
    key_vectors,
    value_vectors,
    head_lambda,
    head_gain,
    residual,
    out_weight,
    mix_gain,
    pre_gain,
    post_gain,
    routes,
    route_weights,
    expert_gate,
    expert_up,
    expert_down,
    shared_gate,
    shared_up,
    shared_down,
):
    n, dp_size = lax.axis_size("sp"), lax.axis_size("dp")
    planes = 4
    inner = n // planes
    tok = queries.shape[1]
    top_count = routes.shape[2]
    cap = 3 * tok * top_count // (2 * n * dp_size)
    cap = (cap + 7) // 8 * 8
    model = residual.shape[2]
    chunks = 4

    q, k, v = to_heads(
        n,
        queries.reshape(tok, -1),
        key_vectors.reshape(tok, -1),
        value_vectors.reshape(tok, -1),
    )
    width = q.shape[2]
    attended = attend(
        q.reshape(-1, width), k.reshape(-1, width), v.reshape(-1, width), head_lambda, head_gain
    )
    flat_heads = to_tokens(n, attended.reshape(n, tok, width))

    mixed_rows = jnp.dot(flat_heads, out_weight, preferred_element_type=jnp.float32)
    updated = (residual[0].astype(jnp.float32) + rms_scale(mixed_rows, mix_gain)).astype(
        jnp.bfloat16
    )
    normed = rms_scale(updated.astype(jnp.float32), pre_gain).astype(jnp.bfloat16)
    side = jnp.concatenate([routes[0].T.astype(jnp.float32), route_weights[0].T], axis=0)
    output = run_experts(
        planes,
        inner,
        dp_size,
        cap,
        chunks,
        normed,
        updated,
        side,
        post_gain.reshape(1, -1),
        (expert_gate[0], expert_up[0], expert_down[0], shared_gate, shared_up, shared_down),
    )
    return output.reshape(1, tok, model)


def solution(mesh):
    in_specs = (
        P("dp", "sp", None, None),
        P("dp", "sp", None, None),
        P("dp", "sp", None, None),
        P("sp"),
        P(),
        P("dp", "sp", None),
        P(),
        P(),
        P(),
        P(),
        P("dp", "sp", None),
        P("dp", "sp", None),
        P(("sp", "dp"), None, None),
        P(("sp", "dp"), None, None),
        P(("sp", "dp"), None, None),
        P(),
        P(),
        P(),
    )
    out_specs = P("dp", "sp", None)
    return jax.shard_map(local, mesh=mesh, in_specs=in_specs, out_specs=out_specs, check_vma=False)
```

time: 199 us -> 171 us (0.86); the launches traced: 195 us -> 171 us
  Pallas kernels: 173 us -> 160 us
  matrix products: 12.6 us -> 4.78 us
  other arithmetic: 5.63 us -> 1.97 us
    pallas_call x1, Pallas kernels: 44.1 us -> 31.8 us  [to_heads(): pl.pallas_call(functools.partial(to_heads_kernel, n), out_shape=[out] * 3...]
    pallas_call x1, Pallas kernels: 110 us -> 101 us  [run_experts(): pl.pallas_call(functools.partial(experts_kernel, planes, inner, dp_size,...]
    pallas_call x1, Pallas kernels: 12.6 us -> 21.3 us  [to_tokens(): pl.pallas_call(functools.partial(to_tokens_kernel, n), out_shape=jax.Shap...]
    dot_general x6 -> x0, matrix products: 7.82 us -> none  [the longest x1 3.39 us: feed_forward(): jnp.dot(hidden, down_w, preferred_element_type=jnp.float32)]
    convert_element_type x4 -> x1, other arithmetic: 3.14 us -> 0.01 us  [local(): routes[0].T.astype(jnp.float32)]
where the time goes in v1:
time: 171 us
  Pallas kernels  160 us (94%)
  matrix products  4.78 us (3%)
  local copies, waits for them, and re-layouts  3.8 us (2%)
  other arithmetic  1.97 us (1%)
    pallas_call x1, Pallas kernels, run_experts(): pl.pallas_call(functools.partial(experts_kernel, planes, inner, dp_size,...  101 us
    pallas_call x1, Pallas kernels, to_heads(): pl.pallas_call(functools.partial(to_heads_kernel, n), out_shape=[out] * 3...  31.8 us
    pallas_call x1, Pallas kernels, to_tokens(): pl.pallas_call(functools.partial(to_tokens_kernel, n), out_shape=jax.Shap...  21.3 us
    pallas_call x1, Pallas kernels, attend(): pl.pallas_call(functools.partial(attend_kernel, min(256, q.shape[0])), ou...  5.8 us
    dot_general x1, matrix products, local(): jnp.dot(flat_heads, out_weight, preferred_element_type=jnp.float32)  4.78 us

profile of v1, /device:TPU:0, one launch (start us, length us, event | category | flops | bytes accessed | tf_op | source)
XLA Modules:
  0.0 170.6 jit_solution(8003011353537635516)
XLA Ops:
  0.0 0.0 copy-start.3
  0.0 0.0 copy-start
  0.0 0.0 copy-start.1
  0.0 1.5 copy_bitcast_fusion
  1.5 0.0 copy-done.3
  1.5 0.1 copy.25
  1.7 31.8 %shard_map.172 = (bf16[8,128,256]{2,1,0:T(8,128)(2,1)S(1)}, bf16[8,128,256]{2,1,0:T(8,128)(2,1)S(1)}, bf16[8,128,256]{2,1,0:T(8,128)(2,1)S(1)}) custom-call(bf16[128,2048]{1,0:T(8,128)(2,1)S(1)} %bitcast.36, bf16[128,2048]{1,0:T(8,128)(2,1)S(1)} %get-tuple-element.16.k_ref, bf16[128,2048]{1,0:T(8,128)(2,1)S(1)} %get-tuple-element.15.v_ref), custom_call_target="tpu_custom_call" | custom-call | tf_op jit(solution)/shard_map/pallas_call | solution.py:97
  33.5 0.0 copy-done
  33.5 0.0 copy-done.1
  33.5 5.8 %shard_map.173 = bf16[1024,256]{1,0:T(8,128)(2,1)S(1)} custom-call(bf16[1024,256]{1,0:T(8,128)(2,1)S(1)} %bitcast.38, bf16[1024,256]{1,0:T(8,128)(2,1)S(1)} %bitcast.39, bf16[1024,256]{1,0:T(8,128)(2,1)S(1)} %bitcast.40, f32[2]{0:T(128)S(1)} %copy-done, f32[1,128]{1,0:T(1,128)S(1)} %bitcast.41), custom_call_target="tpu_custom_call" | custom-call | tf_op jit(solution)/shard_map/pallas_call | solution.py:214
  39.3 21.3 %shard_map.174 = bf16[128,2048]{1,0:T(8,128)(2,1)S(1)} custom-call(bf16[8,128,256]{2,1,0:T(8,128)(2,1)S(1)} %bitcast.37), custom_call_target="tpu_custom_call" | custom-call | tf_op jit(solution)/shard_map/pallas_call | solution.py:146
  60.5 0.0 copy-start.4
  60.6 0.0 copy-start.5
  60.6 4.8 %multiply_reduce_fusion = (f32[128]{0:T(128)S(1)}, f32[128,2048]{1,0:T(8,128)S(1)}) fusion(bf16[128,2048]{1,0:T(8,128)(2,1)S(1)} %shard_map.174, bf16[2048,2048]{1,0:T(8,128)(2,1)} %param.24), kind=kOutput, calls=%fused_computation.7 | convolution fusion | flops 1074265984 | bytes 9961984 | tf_op jit(solution)/shard_map/dot_general | solution.py:724
  65.4 0.0 copy-start.6
  65.4 0.0 copy-start.7
  65.4 0.0 copy-start.8
  65.4 0.0 copy-done.4
  65.4 0.0 copy-done.5
  65.4 0.4 fusion
  65.8 0.0 copy-start.2
  65.8 0.2 copy-done.6
  66.1 1.0 fusion.2.normed_ref
  67.0 0.0 copy-done.7
  67.0 0.0 copy-done.8
  67.0 0.6 pad_maximum_fusion.side_ref
  67.6 0.0 copy-done.2
  67.6 101.1 %shard_map.175 = bf16[128,2048]{1,0:T(8,128)(2,1)} custom-call(bf16[128,2048]{1,0:T(8,128)(2,1)} %fusion.2.normed_ref, bf16[128,2048]{1,0:T(8,128)(2,1)} %copy-done.2, f32[8,128]{1,0:T(8,128)} %pad_maximum_fusion.side_ref, f32[1,2048]{1,0:T(1,128)} %bitcast.49, bf16[2048,512]{1,0:T(8,128)(2,1)} %bitcast.43, bf16[2048,512]{1,0:T(8,128)(2,1)} %bitcast.44, ...), custom_call_target="tpu_custom_call" | custom-call | tf_op jit(solution)/shard_map/pallas_call | solution.py:634
  168.8 1.9 %copy.27 = bf16[1,128,2048]{2,1,0:T(8,128)(2,1)} copy(bf16[1,128,2048]{2,1,0:T(8,128)(2,1)} %bitcast.42) | data formatting | bytes 1048576
  (3 shorter events, 0.0 us)
Async XLA Ops:
  0.0 1.5 copy-start.3
  0.0 33.5 %copy-start = (f32[2]{0:T(128)S(1)}, f32[2]{0:T(128)}, u32[]{:S(2)}) copy-start(f32[2]{0:T(128)} %lam_ref.1) | copy-start | bytes 28
  0.0 33.5 %copy-start.1 = (f32[128]{0:T(128)S(1)}, f32[128]{0:T(128)}, u32[]{:S(2)}) copy-start(f32[128]{0:T(128)} %param.22) | copy-start | bytes 1540
  60.5 4.9 %copy-start.4 = (bf16[1,128,2048]{2,1,0:T(8,128)(2,1)S(1)}, bf16[1,128,2048]{2,1,0:T(8,128)(2,1)}, u32[]{:S(2)}) copy-start(bf16[1,128,2048]{2,1,0:T(8,128)(2,1)} %param.23) | copy-start | bytes 1572868
  60.6 4.9 %copy-start.5 = (f32[2048]{0:T(1024)S(1)}, f32[2048]{0:T(1024)}, u32[]{:S(2)}) copy-start(f32[2048]{0:T(1024)} %param.25) | copy-start | bytes 24580
  65.4 0.7 copy-start.6
  65.4 1.7 copy-start.7
  65.4 1.7 copy-start.8
  65.8 1.9 %copy-start.2 = (bf16[128,2048]{1,0:T(8,128)(2,1)}, bf16[128,2048]{1,0:T(8,128)(2,1)S(1)}, u32[]{:S(2)}) copy-start(bf16[128,2048]{1,0:T(8,128)(2,1)S(1)} %get-tuple-element.12.updated_ref) | copy-start | bytes 1572868

commit v2 on v1

--- a/solution.py
+++ b/solution.py
@@ -37,191 +37,216 @@
     pl.semaphore_wait(barrier, n - 1)
 
 
-def to_heads_kernel(
+def drain(ref, sem):
+    pltpu.make_async_copy(ref, ref, sem).wait()
+
+
+def attend_head(block, which_head, qkv, lam_ref, gain_ref, out):
+    _, _, length, size = qkv.shape
+    half = size // 2
+    lane = lax.broadcasted_iota(jnp.int32, (block, size), 1)
+    row = lax.broadcasted_iota(jnp.int32, (block, block), 0)
+    col = lax.broadcasted_iota(jnp.int32, (block, block), 1)
+    causal = col <= row
+    contract = (((1,), (1,)), ((), ()))
+    q_ref, k_ref, v_ref = (qkv.at[which, which_head] for which in range(3))
+    for step in range(length // block):
+        rows = slice(step * block, (step + 1) * block)
+        past = step * block
+        query = q_ref[rows, :]
+        near, far = [], []
+        for which in range(2):
+            keep = (lane < half) if which == 0 else (lane >= half)
+            part = jnp.where(keep, query, jnp.zeros_like(query))
+            s_near = lax.dot_general(
+                part, k_ref[rows, :], contract, preferred_element_type=jnp.float32
+            ) * (half**-0.5)
+            s_near = jnp.where(causal, s_near, -jnp.inf)
+            top = jnp.max(s_near, axis=-1, keepdims=True)
+            if past:
+                s_far = lax.dot_general(
+                    part, k_ref[:past, :], contract, preferred_element_type=jnp.float32
+                ) * (half**-0.5)
+                top = jnp.maximum(top, jnp.max(s_far, axis=-1, keepdims=True))
+            e_near = jnp.exp(s_near - top)
+            total = jnp.sum(e_near, axis=-1, keepdims=True)
+            if past:
+                e_far = jnp.exp(s_far - top)
+                total = total + jnp.sum(e_far, axis=-1, keepdims=True)
+            scale = 1.0 / total
+            if which == 1:
+                scale = scale * lam_ref[which_head]
+            near.append(e_near * scale)
+            if past:
+                far.append(e_far * scale)
+        mixture = (near[0] - near[1]).astype(jnp.bfloat16)
+        result = jnp.dot(mixture, v_ref[rows, :], preferred_element_type=jnp.float32)
+        if past:
+            mixture = (far[0] - far[1]).astype(jnp.bfloat16)
+            result += jnp.dot(mixture, v_ref[:past, :], preferred_element_type=jnp.float32)
+        out[which_head, rows, :] = rms_scale(result, gain_ref[...]).astype(out.dtype)
+
+
+def attention_kernel(
     n,
     q_ref,
     k_ref,
     v_ref,
-    qo_ref,
-    ko_ref,
-    vo_ref,
+    lam_ref,
+    head_gain_ref,
+    residual_ref,
+    mix_gain_ref,
+    pre_gain_ref,
+    weight_hbm,
+    updated_ref,
+    normed_ref,
+    weight,
+    qkv,
+    out,
+    heads_in,
+    mixed,
+    load_sem,
     send_sem,
     recv_sem,
-    own_sem,
+    back_send,
+    back_recv,
 ):
     me = lax.axis_index("sp")
-    width = qo_ref.shape[2]
-    pairs = ((q_ref, qo_ref), (k_ref, ko_ref), (v_ref, vo_ref))
+    _, heads, length, size = qkv.shape
+    tok = length // n
+    model = updated_ref.shape[1]
+    way = 1 - 2 * (me // (n // 2))
     line_barrier(n, me)
 
-    def copy(which, off):
-        source, target = pairs[which]
-        dst = lax.rem(me + off, n)
+    def loop(first, stop, action):
+        lax.fori_loop(first, stop, lambda i, carry: (action(i), carry)[1], 0)
+
+    def spot(index):
+        return pl.ds(pl.multiple_of(index * tok, tok), tok)
+
+    def to_head(head, which, off):
+        dst = lax.rem(me + way * off + n, n)
         return pltpu.make_async_remote_copy(
-            src_ref=source.at[:, columns_of(dst, width)],
-            dst_ref=target.at[me],
-            send_sem=send_sem.at[which, off],
-            recv_sem=recv_sem.at[which, off],
+            src_ref=(q_ref, k_ref, v_ref)[which].at[:, columns_of(dst * heads + head, size)],
+            dst_ref=qkv.at[which, head, spot(me)],
+            send_sem=send_sem.at[head],
+            recv_sem=recv_sem.at[head],
             device_id={"sp": dst},
             device_id_type=MESH,
         )
 
-    def own(which):
-        source, target = pairs[which]
+    def to_token(head, off):
+        dst = lax.rem(me + way * off + n, n)
+        return pltpu.make_async_remote_copy(
+            src_ref=out.at[head, spot(dst)],
+            dst_ref=heads_in.at[head, :, columns_of(me, size)],
+            send_sem=back_send.at[head],
+            recv_sem=back_recv.at[head],
+            device_id={"sp": dst},
+            device_id_type=MESH,
+        )
+
+    def start_head(head):
+        def one(off):
+            for which in range(3):
+                to_head(head, which, off).start()
+
+        loop(1, n, one)
+
+    for head in range(heads):
+        start_head(head)
+
+    def load(head, index):
         return pltpu.make_async_copy(
-            source.at[:, columns_of(me, width)], target.at[me], own_sem.at[which]
-        )
-
-    def start(off, carry):
-        for which in range(3):
-            copy(which, off).start()
-        return carry
-
-    def finish(off, carry):
-        for which in range(3):
-            copy(which, off).wait()
-        return carry
-
-    lax.fori_loop(1, n, start, 0)
-    for which in range(3):
-        own(which).start()
-    for which in range(3):
-        own(which).wait()
-    lax.fori_loop(1, n, finish, 0)
-
-
-def to_heads(n, q, k, v):
+            weight_hbm.at[pl.ds(pl.multiple_of((index * heads + head) * size, size), size)],
+            weight.at[head, pl.ds(pl.multiple_of(index * size, size), size)],
+            load_sem.at[head],
+        )
+
+    for head in range(heads):
+        loop(0, n, lambda index: load(head, index).start())
+        for which, source in enumerate((q_ref, k_ref, v_ref)):
+            qkv[which, head, spot(me), :] = source[:, columns_of(me * heads + head, size)]
+
+    rest = pl.ds(0, (n - 1) * tok)
+
+    def arrived(head):
+        drain(qkv.at[:, head, rest], recv_sem.at[head])
+
+    for head in range(heads):
+        arrived(head)
+        attend_head(min(256, length), head, qkv, lam_ref, head_gain_ref, out)
+        loop(1, n, lambda off: to_token(head, off).start())
+        heads_in[head, :, columns_of(me, size)] = out[head, spot(me), :]
+
+    tile = min(512, model)
+    for head in range(heads):
+        drain(weight.at[head], load_sem.at[head])
+        drain(out.at[head, rest], back_recv.at[head])
+
+        def project(index):
+            some = columns_of(index, tile)
+            value = jnp.dot(
+                heads_in[head], weight[head, :, some], preferred_element_type=jnp.float32
+            )
+            if head:
+                mixed[:, some] += value
+            else:
+                mixed[:, some] = value
+
+        loop(0, model // tile, project)
+
+    value = residual_ref[...].astype(jnp.float32) + rms_scale(mixed[...], mix_gain_ref[...])
+    updated_ref[...] = value.astype(updated_ref.dtype)
+    normed_ref[...] = rms_scale(
+        updated_ref[...].astype(jnp.float32), pre_gain_ref[...]
+    ).astype(normed_ref.dtype)
+    for head in range(heads):
+        drain(qkv.at[:, head, rest], send_sem.at[head])
+        drain(out.at[head, rest], back_send.at[head])
+
+
+def run_attention(n, q, k, v, head_lambda, head_gain, residual, mix_gain, pre_gain, weight):
     tok, model = q.shape
-    width = model // n
-    out = jax.ShapeDtypeStruct((n, tok, width), q.dtype)
+    size = head_gain.shape[0]
+    heads = model // n // size
+    kind = q.dtype
+    dma = pltpu.SemaphoreType.DMA
+    shape = jax.ShapeDtypeStruct((tok, model), kind)
     return pl.pallas_call(
-        functools.partial(to_heads_kernel, n),
-        out_shape=[out] * 3,
-        in_specs=[VMEM] * 3,
-        out_specs=[VMEM] * 3,
+        functools.partial(attention_kernel, n),
+        out_shape=[shape, shape],
+        in_specs=[VMEM] * 3
+        + [pl.BlockSpec(memory_space=pltpu.SMEM)]
+        + [VMEM] * 4
+        + [pl.BlockSpec(memory_space=pl.ANY)],
+        out_specs=[VMEM] * 2,
         scratch_shapes=[
-            pltpu.SemaphoreType.DMA((3, n)),
-            pltpu.SemaphoreType.DMA((3, n)),
-            pltpu.SemaphoreType.DMA((3,)),
+            pltpu.VMEM((heads, n * size, model), kind),
+            pltpu.VMEM((3, heads, n * tok, size), kind),
+            pltpu.VMEM((heads, n * tok, size), kind),
+            pltpu.VMEM((heads, tok, n * size), kind),
+            pltpu.VMEM((tok, model), jnp.float32),
+            dma((heads,)),
+            dma((heads,)),
+            dma((heads,)),
+            dma((heads,)),
+            dma((heads,)),
         ],
         compiler_params=pltpu.CompilerParams(
-            collective_id=0, has_side_effects=True, vmem_limit_bytes=32 * 2**20
+            collective_id=0, has_side_effects=True, vmem_limit_bytes=56 * 2**20
         ),
-    )(q, k, v)
-
-
-def to_tokens_kernel(n, a_ref, o_ref, send_sem, recv_sem, own_sem):
-    me = lax.axis_index("sp")
-    width = a_ref.shape[2]
-    line_barrier(n, me)
-
-    def copy(off):
-        dst = lax.rem(me + off, n)
-        return pltpu.make_async_remote_copy(
-            src_ref=a_ref.at[dst],
-            dst_ref=o_ref.at[:, columns_of(me, width)],
-            send_sem=send_sem.at[off],
-            recv_sem=recv_sem.at[off],
-            device_id={"sp": dst},
-            device_id_type=MESH,
-        )
-
-    def start(off, carry):
-        copy(off).start()
-        return carry
-
-    def finish(off, carry):
-        copy(off).wait()
-        return carry
-
-    lax.fori_loop(1, n, start, 0)
-    own = pltpu.make_async_copy(a_ref.at[me], o_ref.at[:, columns_of(me, width)], own_sem)
-    own.start()
-    own.wait()
-    lax.fori_loop(1, n, finish, 0)
-
-
-def to_tokens(n, attended):
-    _, tok, width = attended.shape
-    return pl.pallas_call(
-        functools.partial(to_tokens_kernel, n),
-        out_shape=jax.ShapeDtypeStruct((tok, n * width), attended.dtype),
-        in_specs=[VMEM],
-        out_specs=VMEM,
-        scratch_shapes=[
-            pltpu.SemaphoreType.DMA((n,)),
-            pltpu.SemaphoreType.DMA((n,)),
-            pltpu.SemaphoreType.DMA,
-        ],
-        compiler_params=pltpu.CompilerParams(
-            collective_id=1, has_side_effects=True, vmem_limit_bytes=32 * 2**20
-        ),
-    )(attended)
-
-
-def attend_kernel(block, q_ref, k_ref, v_ref, lam_ref, gain_ref, o_ref):
-    length, width = q_ref.shape
-    value_size = gain_ref.shape[1]
-    heads = width // value_size
-    half = value_size // 2
-    lane = lax.broadcasted_iota(jnp.int32, (block, value_size), 1)
-    row = lax.broadcasted_iota(jnp.int32, (block, block), 0)
-    col = lax.broadcasted_iota(jnp.int32, (block, block), 1)
-    causal = col <= row
-    contract = (((1,), (1,)), ((), ()))
-    for head in range(heads):
-        cols = slice(head * value_size, (head + 1) * value_size)
-        for step in range(length // block):
-            rows = slice(step * block, (step + 1) * block)
-            past = step * block
-            query = q_ref[rows, cols]
-            near, far = [], []
-            for which in range(2):
-                keep = (lane < half) if which == 0 else (lane >= half)
-                part = jnp.where(keep, query, jnp.zeros_like(query))
-                s_near = lax.dot_general(
-                    part, k_ref[rows, cols], contract, preferred_element_type=jnp.float32
-                ) * (half**-0.5)
-                s_near = jnp.where(causal, s_near, -jnp.inf)
-                top = jnp.max(s_near, axis=-1, keepdims=True)
-                if past:
-                    s_far = lax.dot_general(
-                        part, k_ref[:past, cols], contract, preferred_element_type=jnp.float32
-                    ) * (half**-0.5)
-                    top = jnp.maximum(top, jnp.max(s_far, axis=-1, keepdims=True))
-                e_near = jnp.exp(s_near - top)
-                total = jnp.sum(e_near, axis=-1, keepdims=True)
-                if past:
-                    e_far = jnp.exp(s_far - top)
-                    total = total + jnp.sum(e_far, axis=-1, keepdims=True)
-                scale = 1.0 / total
-                if which == 1:
-                    scale = scale * lam_ref[head]
-                near.append(e_near * scale)
-                if past:
-                    far.append(e_far * scale)
-            mixture = (near[0] - near[1]).astype(jnp.bfloat16)
-            result = jnp.dot(mixture, v_ref[rows, cols], preferred_element_type=jnp.float32)
-            if past:
-                mixture = (far[0] - far[1]).astype(jnp.bfloat16)
-                result += jnp.dot(
-                    mixture, v_ref[:past, cols], preferred_element_type=jnp.float32
-                )
-            o_ref[rows, cols] = rms_scale(result, gain_ref[...]).astype(o_ref.dtype)
-
-
-def attend(q, k, v, head_lambda, head_gain):
-    return pl.pallas_call(
-        functools.partial(attend_kernel, min(256, q.shape[0])),
-        out_shape=jax.ShapeDtypeStruct(q.shape, q.dtype),
-        in_specs=[VMEM] * 3 + [pl.BlockSpec(memory_space=pltpu.SMEM), VMEM],
-        out_specs=VMEM,
-        compiler_params=pltpu.CompilerParams(vmem_limit_bytes=48 * 2**20),
-    )(q, k, v, head_lambda, head_gain.reshape(1, -1))
-
-
-def drain(ref, sem):
-    pltpu.make_async_copy(ref, ref, sem).wait()
+    )(
+        q,
+        k,
+        v,
+        head_lambda,
+        head_gain.reshape(1, -1),
+        residual,
+        mix_gain.reshape(1, -1),
+        pre_gain.reshape(1, -1),
+        weight,
+    )
 
 
 def experts_kernel(
@@ -709,23 +734,18 @@
     model = residual.shape[2]
     chunks = 4
 
-    q, k, v = to_heads(
+    updated, normed = run_attention(
         n,
         queries.reshape(tok, -1),
         key_vectors.reshape(tok, -1),
         value_vectors.reshape(tok, -1),
+        head_lambda,
+        head_gain,
+        residual[0],
+        mix_gain,
+        pre_gain,
+        out_weight,
     )
-    width = q.shape[2]
-    attended = attend(
-        q.reshape(-1, width), k.reshape(-1, width), v.reshape(-1, width), head_lambda, head_gain
-    )
-    flat_heads = to_tokens(n, attended.reshape(n, tok, width))
-
-    mixed_rows = jnp.dot(flat_heads, out_weight, preferred_element_type=jnp.float32)
-    updated = (residual[0].astype(jnp.float32) + rms_scale(mixed_rows, mix_gain)).astype(
-        jnp.bfloat16
-    )
-    normed = rms_scale(updated.astype(jnp.float32), pre_gain).astype(jnp.bfloat16)
     side = jnp.concatenate([routes[0].T.astype(jnp.float32), route_weights[0].T], axis=0)
     output = run_experts(
         planes,

time: 171 us -> 159 us (0.930)
  Pallas kernels: 160 us -> 153 us
  matrix products: 4.78 us -> 0 us
    pallas_call x1, Pallas kernels: 101 us -> 93.6 us  [run_experts(): pl.pallas_call(functools.partial(experts_kernel, planes, inner, dp_size,...]
    dot_general x1 -> x0, matrix products: 4.78 us -> none  [local(): jnp.dot(flat_heads, out_weight, preferred_element_type=jnp.float32)]
    pallas_call x3 -> x1, Pallas kernels: 58.8 us -> 59 us  [run_attention(): pl.pallas_call(functools.partial(attention_kernel, n), out_shape=[shape,...]
where the time goes in v2:
time: 159 us
  Pallas kernels  153 us (96%)
  local copies, waits for them, and re-layouts  5.33 us (3%)
    pallas_call x1, Pallas kernels, run_experts(): pl.pallas_call(functools.partial(experts_kernel, planes, inner, dp_size,...  93.6 us
    pallas_call x1, Pallas kernels, run_attention(): pl.pallas_call(functools.partial(attention_kernel, n), out_shape=[shape,...  59 us

profile of v2, /device:TPU:0, one launch (start us, length us, event | category | flops | bytes accessed | tf_op | source)
XLA Modules:
  0.0 158.6 jit_solution(11474325185584475090)
XLA Ops:
  0.0 0.0 copy-start
  0.0 2.5 %copy_bitcast_fusion = (bf16[128,2048]{1,0:T(8,128)(2,1)}, bf16[128,2048]{1,0:T(8,128)(2,1)}) fusion(bf16[16,8,16,128]{3,2,1,0:T(8,128)(2,1)} %bitcast.35, bf16[16,8,16,128]{3,2,1,0:T(8,128)(2,1)} %bitcast.36), kind=kLoop, calls=%fused_computation | loop fusion | bytes 2097152 | tf_op jit(solution)/shard_map/reshape | solution.py:741
  2.5 0.0 copy-done
  2.5 0.9 copy.25
  3.4 0.0 copy-start.1
  3.4 0.0 copy-start.2
  3.4 59.0 %shard_map.172 = (bf16[128,2048]{1,0:T(8,128)(2,1)}, bf16[128,2048]{1,0:T(8,128)(2,1)}) custom-call(bf16[128,2048]{1,0:T(8,128)(2,1)} %bitcast.33, bf16[128,2048]{1,0:T(8,128)(2,1)} %get-tuple-element.10.k_ref, bf16[128,2048]{1,0:T(8,128)(2,1)} %get-tuple-element.9.v_ref, f32[2]{0:T(128)} %lam_ref.1, f32[1,128]{1,0:T(1,128)} %bitcast.42, ...), custom_call_target="tpu_custom_call" | custom-call | tf_op jit(solution)/shard_map/pallas_call | solution.py:216
  62.5 0.0 copy-done.1
  62.5 0.0 copy-done.2
  62.5 0.6 pad_maximum_fusion.side_ref
  63.1 93.6 %shard_map.173 = bf16[128,2048]{1,0:T(8,128)(2,1)} custom-call(bf16[128,2048]{1,0:T(8,128)(2,1)} %get-tuple-element.7.normed_ref, bf16[128,2048]{1,0:T(8,128)(2,1)} %get-tuple-element.8.updated_ref, f32[8,128]{1,0:T(8,128)} %pad_maximum_fusion.side_ref, f32[1,2048]{1,0:T(1,128)} %bitcast.38, bf16[2048,512]{1,0:T(8,128)(2,1)} %bitcast.30, ...), custom_call_target="tpu_custom_call" | custom-call | tf_op jit(solution)/shard_map/pallas_call | solution.py:659
  156.8 1.9 %copy.27 = bf16[1,128,2048]{2,1,0:T(8,128)(2,1)} copy(bf16[1,128,2048]{2,1,0:T(8,128)(2,1)} %bitcast.29) | data formatting | bytes 1048576
  (1 shorter events, 0.0 us)
Async XLA Ops:
  0.0 2.5 %copy-start = (bf16[1,128,16,128]{3,2,1,0:T(8,128)(2,1)S(1)}, bf16[1,128,16,128]{3,2,1,0:T(8,128)(2,1)}, u32[]{:S(2)}) copy-start(bf16[1,128,16,128]{3,2,1,0:T(8,128)(2,1)} %param.18) | copy-start | bytes 1572868
  3.4 59.0 %copy-start.1 = (s32[1,128,4]{1,2,0:T(4,128)S(1)}, s32[1,128,4]{1,2,0:T(4,128)}, u32[]{:S(2)}) copy-start(s32[1,128,4]{1,2,0:T(4,128)} %param.28) | copy-start | bytes 6148
  3.4 59.1 %copy-start.2 = (f32[1,128,4]{1,2,0:T(4,128)S(1)}, f32[1,128,4]{1,2,0:T(4,128)}, u32[]{:S(2)}) copy-start(f32[1,128,4]{1,2,0:T(4,128)} %param.29) | copy-start | bytes 6148

commit v3 on v2

--- a/solution.py
+++ b/solution.py
@@ -405,7 +405,10 @@
 
         over(1, group, one)
 
-    def give_back(slot, chunk):
+    def give_back(slot, first, stop):
+        over(first, stop, lambda chunk: give_chunk(slot, chunk))
+
+    def give_chunk(slot, chunk):
         def one(k):
             there, device = peer(k)
             pltpu.make_async_remote_copy(
@@ -458,7 +461,7 @@
         inbox[slot, chunk, place] = rows[slot, chunk, place]
         deal(slot, chunk)
 
-    def collect(slot):
+    def collect(slot, first, stop):
         block = block_of(slot)
 
         def one(chunk):
@@ -466,7 +469,7 @@
             pushes(block, False, lambda up: push(block, chunk, up).start())
             pick_rows(slot, block, chunk)
 
-        over(0, chunks, one)
+        over(first, stop, one)
 
     tile = min(256, gate_w.shape[1])
     tiles = gate_w.shape[1] // tile
@@ -497,14 +500,20 @@
             outs[slot, chunk] = value.reshape(group, cap, width).astype(outs.dtype)
             landed[slot, chunk, place] = outs[slot, chunk, place]
             if send:
-                give_back(slot, chunk)
+                give_chunk(slot, chunk)
 
         over(0, chunks, one)
 
     contract = (((0,), (0,)), ((), ()))
 
+    def wait_landed(slot, first, stop):
+        over(
+            first,
+            stop,
+            lambda chunk: drain(others(landed, slot, chunk), back_recv.at[slot, chunk]),
+        )
+
     def combine(slot, chunk):
-        drain(others(landed, slot, chunk), back_recv.at[slot, chunk])
         block = landed[slot, chunk].astype(jnp.float32).reshape(group * cap, width)
         block = block.astype(jnp.bfloat16)
         value = lax.dot_general(high[slot], block, contract, preferred_element_type=jnp.float32)
@@ -545,8 +554,8 @@
         def _():
             pass_sum(slot, block, chunk, 0).start()
 
-    def reduce_all(slot):
-        over(0, chunks, lambda chunk: reduce_one(slot, block_of(slot), chunk))
+    def reduce_some(slot, first, stop):
+        over(first, stop, lambda chunk: reduce_one(slot, block_of(slot), chunk))
 
     for chunk in range(chunks):
         tokens[z, chunk] = normed_ref[:, chunk * width : (chunk + 1) * width]
@@ -558,52 +567,85 @@
     tables(0, side_ref[...])
     over(0, chunks, lambda chunk: pick_rows(0, z, chunk))
 
-    for load in loads[:3]:
-        load.wait()
-    shared = hidden.at[pl.ds(0, tok)]
-    hidden_of(normed_ref, sgate_w, sup_w, shared)
-
-    def shared_down(chunk):
-        value = jnp.dot(
-            shared[...], sdown_w[:, columns_of(chunk, width)], preferred_element_type=jnp.float32
-        )
-        total[chunk] = value.astype(jnp.bfloat16).astype(jnp.float32)
-
-    over(0, chunks, shared_down)
     for slot in range(1, planes):
         block = block_of(slot)
         drain(sides.at[block], side_recv.at[block])
         tables(slot, sides[block])
-    collect(1)
-    for load in loads[3:]:
+    shared = hidden.at[pl.ds(0, tok)]
+    part = max(1, chunks // 2)
+
+    def run_shared():
+        hidden_of(normed_ref, sgate_w, sup_w, shared)
+
+        def one(chunk):
+            value = jnp.dot(
+                shared[...],
+                sdown_w[:, columns_of(chunk, width)],
+                preferred_element_type=jnp.float32,
+            )
+            total[chunk] = value.astype(jnp.bfloat16).astype(jnp.float32)
+
+        over(0, chunks, one)
+
+    collect(1, 0, chunks)
+    for load in loads:
         load.wait()
-    expert(0, False)
-    collect(2)
-    expert(1, True)
-    collect(3)
-    expert(2, True)
 
     @pl.when(is_end)
     def _():
-        reduce_all(1)
-
-    expert(3, True)
-    over(0, chunks, lambda chunk: give_back(0, chunk))
-
-    @pl.when(is_end)
-    def _():
-        reduce_all(2)
-        reduce_all(3)
+        collect(2, 0, 1)
+        expert(1, False)
+        give_back(1, 0, part)
+        collect(2, 1, chunks)
+        expert(0, False)
+        collect(3, 0, part)
+        wait_landed(1, 0, part)
+        reduce_some(1, 0, part)
+        collect(3, part, chunks)
+        expert(2, False)
+        run_shared()
+        expert(3, True)
+        give_back(2, 0, chunks)
+        wait_landed(3, 0, part)
+        reduce_some(3, 0, part)
+        wait_landed(3, part, chunks)
+        reduce_some(3, part, chunks)
+        give_back(1, part, chunks)
+        wait_landed(2, 0, part)
+        reduce_some(2, 0, part)
+        wait_landed(2, part, chunks)
+        reduce_some(2, part, chunks)
+        give_back(0, 0, chunks)
+        wait_landed(1, part, chunks)
+        reduce_some(1, part, chunks)
 
     @pl.when(jnp.logical_not(is_end))
     def _():
-        reduce_all(1)
+        collect(2, 0, chunks)
+        expert(0, False)
+        collect(3, 0, part)
+        expert(1, False)
+        collect(3, part, chunks)
+        expert(2, False)
+        expert(3, True)
+        give_back(2, 0, chunks)
+        give_back(1, 0, chunks)
+        give_back(0, 0, chunks)
+        run_shared()
+        wait_landed(3, 0, chunks)
+        wait_landed(2, 0, chunks)
 
         def one(chunk):
             reduce_one(3, block_of(3), chunk)
             reduce_one(2, block_of(2), chunk)
 
-        over(0, chunks, one)
+        over(0, chunks - 1, one)
+        wait_landed(1, 0, chunks)
+        reduce_some(1, 0, 1)
+        over(chunks - 1, chunks, one)
+        reduce_some(1, 1, chunks)
+
+    wait_landed(0, 0, chunks)
 
     def settle(chunk):
         total[chunk] += combine(0, chunk)

time: 159 us -> 154 us (0.969); the launches traced: 159 us -> 151 us
  Pallas kernels: 153 us -> 146 us
    pallas_call x1, Pallas kernels: 93.6 us -> 86.5 us  [run_experts(): pl.pallas_call(functools.partial(experts_kernel, planes, inner, dp_size,...]
where the time goes in v3:
time: 154 us; the launch traced here: 151 us
  Pallas kernels  146 us (95%)
  local copies, waits for them, and re-layouts  5.33 us (3%)
    pallas_call x1, Pallas kernels, run_experts(): pl.pallas_call(functools.partial(experts_kernel, planes, inner, dp_size,...  86.5 us
    pallas_call x1, Pallas kernels, run_attention(): pl.pallas_call(functools.partial(attention_kernel, n), out_shape=[shape,...  59 us

profile of v3, /device:TPU:0, one launch (start us, length us, event | category | flops | bytes accessed | tf_op | source)
XLA Modules:
  0.0 151.5 jit_solution(17602174941673031557)
XLA Ops:
  0.0 0.0 copy-start
  0.0 2.5 %copy_bitcast_fusion = (bf16[128,2048]{1,0:T(8,128)(2,1)}, bf16[128,2048]{1,0:T(8,128)(2,1)}) fusion(bf16[16,8,16,128]{3,2,1,0:T(8,128)(2,1)} %bitcast.35, bf16[16,8,16,128]{3,2,1,0:T(8,128)(2,1)} %bitcast.36), kind=kLoop, calls=%fused_computation | loop fusion | bytes 2097152 | tf_op jit(solution)/shard_map/reshape | solution.py:783
  2.5 0.0 copy-done
  2.5 0.9 copy.25
  3.4 0.0 copy-start.1
  3.4 0.0 copy-start.2
  3.4 59.0 %shard_map.172 = (bf16[128,2048]{1,0:T(8,128)(2,1)}, bf16[128,2048]{1,0:T(8,128)(2,1)}) custom-call(bf16[128,2048]{1,0:T(8,128)(2,1)} %bitcast.33, bf16[128,2048]{1,0:T(8,128)(2,1)} %get-tuple-element.10.k_ref, bf16[128,2048]{1,0:T(8,128)(2,1)} %get-tuple-element.9.v_ref, f32[2]{0:T(128)} %lam_ref.1, f32[1,128]{1,0:T(1,128)} %bitcast.42, ...), custom_call_target="tpu_custom_call" | custom-call | tf_op jit(solution)/shard_map/pallas_call | solution.py:216
  62.5 0.0 copy-done.1
  62.5 0.0 copy-done.2
  62.5 0.6 pad_maximum_fusion.side_ref
  63.1 86.5 %shard_map.173 = bf16[128,2048]{1,0:T(8,128)(2,1)} custom-call(bf16[128,2048]{1,0:T(8,128)(2,1)} %get-tuple-element.7.normed_ref, bf16[128,2048]{1,0:T(8,128)(2,1)} %get-tuple-element.8.updated_ref, f32[8,128]{1,0:T(8,128)} %pad_maximum_fusion.side_ref, f32[1,2048]{1,0:T(1,128)} %bitcast.38, bf16[2048,512]{1,0:T(8,128)(2,1)} %bitcast.30, ...), custom_call_target="tpu_custom_call" | custom-call | tf_op jit(solution)/shard_map/pallas_call | solution.py:701
  149.6 1.9 %copy.27 = bf16[1,128,2048]{2,1,0:T(8,128)(2,1)} copy(bf16[1,128,2048]{2,1,0:T(8,128)(2,1)} %bitcast.29) | data formatting | bytes 1048576
  (1 shorter events, 0.0 us)
Async XLA Ops:
  0.0 2.5 %copy-start = (bf16[1,128,16,128]{3,2,1,0:T(8,128)(2,1)S(1)}, bf16[1,128,16,128]{3,2,1,0:T(8,128)(2,1)}, u32[]{:S(2)}) copy-start(bf16[1,128,16,128]{3,2,1,0:T(8,128)(2,1)} %param.18) | copy-start | bytes 1572868
  3.4 59.0 %copy-start.1 = (s32[1,128,4]{1,2,0:T(4,128)S(1)}, s32[1,128,4]{1,2,0:T(4,128)}, u32[]{:S(2)}) copy-start(s32[1,128,4]{1,2,0:T(4,128)} %param.28) | copy-start | bytes 6148
  3.4 59.1 %copy-start.2 = (f32[1,128,4]{1,2,0:T(4,128)S(1)}, f32[1,128,4]{1,2,0:T(4,128)}, u32[]{:S(2)}) copy-start(f32[1,128,4]{1,2,0:T(4,128)} %param.29) | copy-start | bytes 6148

commit v4 on v3

--- a/solution.py
+++ b/solution.py
@@ -22,19 +22,6 @@
 
 def columns_of(index, width):
     return pl.ds(pl.multiple_of(index * width, width), width)
-
-
-def line_barrier(n, me):
-    barrier = pltpu.get_barrier_semaphore()
-
-    def greet(off, carry):
-        pl.semaphore_signal(
-            barrier, inc=1, device_id={"sp": lax.rem(me + off, n)}, device_id_type=MESH
-        )
-        return carry
-
-    lax.fori_loop(1, n, greet, 0)
-    pl.semaphore_wait(barrier, n - 1)
 
 
 def drain(ref, sem):
@@ -87,7 +74,8 @@
         out[which_head, rows, :] = rms_scale(result, gain_ref[...]).astype(out.dtype)
 
 
-def attention_kernel(
+def attention_part(
+    meanwhile,
     n,
     q_ref,
     k_ref,
@@ -116,7 +104,6 @@
     tok = length // n
     model = updated_ref.shape[1]
     way = 1 - 2 * (me // (n // 2))
-    line_barrier(n, me)
 
     def loop(first, stop, action):
         lax.fori_loop(first, stop, lambda i, carry: (action(i), carry)[1], 0)
@@ -168,6 +155,7 @@
         for which, source in enumerate((q_ref, k_ref, v_ref)):
             qkv[which, head, spot(me), :] = source[:, columns_of(me * heads + head, size)]
 
+    meanwhile()
     rest = pl.ds(0, (n - 1) * tok)
 
     def arrived(head):
@@ -201,62 +189,30 @@
     normed_ref[...] = rms_scale(
         updated_ref[...].astype(jnp.float32), pre_gain_ref[...]
     ).astype(normed_ref.dtype)
-    for head in range(heads):
-        drain(qkv.at[:, head, rest], send_sem.at[head])
-        drain(out.at[head, rest], back_send.at[head])
-
-
-def run_attention(n, q, k, v, head_lambda, head_gain, residual, mix_gain, pre_gain, weight):
-    tok, model = q.shape
-    size = head_gain.shape[0]
-    heads = model // n // size
-    kind = q.dtype
-    dma = pltpu.SemaphoreType.DMA
-    shape = jax.ShapeDtypeStruct((tok, model), kind)
-    return pl.pallas_call(
-        functools.partial(attention_kernel, n),
-        out_shape=[shape, shape],
-        in_specs=[VMEM] * 3
-        + [pl.BlockSpec(memory_space=pltpu.SMEM)]
-        + [VMEM] * 4
-        + [pl.BlockSpec(memory_space=pl.ANY)],
-        out_specs=[VMEM] * 2,
-        scratch_shapes=[
-            pltpu.VMEM((heads, n * size, model), kind),
-            pltpu.VMEM((3, heads, n * tok, size), kind),
-            pltpu.VMEM((heads, n * tok, size), kind),
-            pltpu.VMEM((heads, tok, n * size), kind),
-            pltpu.VMEM((tok, model), jnp.float32),
-            dma((heads,)),
-            dma((heads,)),
-            dma((heads,)),
-            dma((heads,)),
-            dma((heads,)),
-        ],
-        compiler_params=pltpu.CompilerParams(
-            collective_id=0, has_side_effects=True, vmem_limit_bytes=56 * 2**20
-        ),
-    )(
-        q,
-        k,
-        v,
-        head_lambda,
-        head_gain.reshape(1, -1),
-        residual,
-        mix_gain.reshape(1, -1),
-        pre_gain.reshape(1, -1),
-        weight,
-    )
-
-
-def experts_kernel(
+
+    def finish():
+        for head in range(heads):
+            drain(qkv.at[:, head, rest], send_sem.at[head])
+            drain(out.at[head, rest], back_send.at[head])
+
+    return finish
+
+
+def layer_kernel(
     planes,
     inner,
     dp_size,
     chunks,
     top,
-    normed_ref,
-    updated_ref,
+    q_ref,
+    k_ref,
+    v_ref,
+    lam_ref,
+    head_gain_ref,
+    residual_ref,
+    mix_gain_ref,
+    pre_gain_ref,
+    weight_hbm,
     side_ref,
     gain_ref,
     gate_hbm,
@@ -266,6 +222,18 @@
     sup_hbm,
     sdown_hbm,
     o_ref,
+    normed_ref,
+    updated_ref,
+    weight,
+    qkv,
+    head_out,
+    heads_in,
+    mixed,
+    w_sem,
+    q_send,
+    q_recv,
+    h_send,
+    h_recv,
     gate_w,
     up_w,
     down_w,
@@ -333,11 +301,15 @@
             barrier, inc=1, device_id=peer(k)[1], device_id_type=MESH
         ),
     )
-    for d in range(1, planes):
-        pl.semaphore_signal(
-            barrier, inc=1, device_id=column(lax.rem(z + d, planes)), device_id_type=MESH
-        )
-    pl.semaphore_wait(barrier, group - 1 + planes - 1)
+    n = planes * inner
+    over(
+        1,
+        n,
+        lambda k: pl.semaphore_signal(
+            barrier, inc=1, device_id={"sp": lax.rem(sp + k, n)}, device_id_type=MESH
+        ),
+    )
+    pl.semaphore_wait(barrier, group - 1 + n - 1)
 
     loads = [
         pltpu.make_async_copy(source, target, load_sem.at[index])
@@ -557,20 +529,46 @@
     def reduce_some(slot, first, stop):
         over(first, stop, lambda chunk: reduce_one(slot, block_of(slot), chunk))
 
+    def meanwhile():
+        for d in range(1, planes):
+            side(d).start()
+        for load in loads:
+            load.start()
+        tables(0, side_ref[...])
+        for slot in range(1, planes):
+            block = block_of(slot)
+            drain(sides.at[block], side_recv.at[block])
+            tables(slot, sides[block])
+
+    finish = attention_part(
+        meanwhile,
+        n,
+        q_ref,
+        k_ref,
+        v_ref,
+        lam_ref,
+        head_gain_ref,
+        residual_ref,
+        mix_gain_ref,
+        pre_gain_ref,
+        weight_hbm,
+        updated_ref,
+        normed_ref,
+        weight,
+        qkv,
+        head_out,
+        heads_in,
+        mixed,
+        w_sem,
+        q_send,
+        q_recv,
+        h_send,
+        h_recv,
+    )
     for chunk in range(chunks):
         tokens[z, chunk] = normed_ref[:, chunk * width : (chunk + 1) * width]
-    for d in range(1, planes):
-        side(d).start()
     over(0, chunks, lambda chunk: pushes(z, True, lambda up: push(z, chunk, up).start()))
-    for load in loads:
-        load.start()
-    tables(0, side_ref[...])
     over(0, chunks, lambda chunk: pick_rows(0, z, chunk))
-
-    for slot in range(1, planes):
-        block = block_of(slot)
-        drain(sides.at[block], side_recv.at[block])
-        tables(slot, sides[block])
     shared = hidden.at[pl.ds(0, tok)]
     part = max(1, chunks // 2)
 
@@ -672,6 +670,7 @@
             updated_ref[:, some].astype(jnp.float32) + total[chunk] * scale * gain_ref[:, some]
         ).astype(o_ref.dtype)
 
+    finish()
     for d in range(1, planes):
         side(d).wait_send()
 
@@ -687,25 +686,45 @@
     over(0, chunks, sent)
 
 
-def run_experts(planes, inner, dp_size, cap, chunks, normed, updated, side, gain, weights):
+def run_layer(planes, inner, dp_size, cap, chunks, qkv, head_params, rows, out_weight, side, gain, weights):
     group = inner * dp_size
-    tok, model = normed.shape
+    n = planes * inner
+    tok, model = qkv[0].shape
     ff = weights[0].shape[1]
+    size = head_params[1].shape[1]
+    heads = model // n // size
     width = model // chunks
-    kind = normed.dtype
+    kind = qkv[0].dtype
     blocks = pltpu.VMEM((planes, chunks, group, cap, width), kind)
     columns = pltpu.VMEM((planes, chunks, tok, width), kind)
     table = pltpu.VMEM((planes, group * cap, tok), kind)
     wide, tall = pltpu.VMEM((model, ff), kind), pltpu.VMEM((ff, model), kind)
+    flat = pltpu.VMEM((tok, model), kind)
     dma = pltpu.SemaphoreType.DMA
+    anywhere = pl.BlockSpec(memory_space=pl.ANY)
     return pl.pallas_call(
-        functools.partial(
-            experts_kernel, planes, inner, dp_size, chunks, side.shape[0] // 2
-        ),
+        functools.partial(layer_kernel, planes, inner, dp_size, chunks, side.shape[0] // 2),
         out_shape=jax.ShapeDtypeStruct((tok, model), kind),
-        in_specs=[VMEM] * 4 + [pl.BlockSpec(memory_space=pl.ANY)] * 6,
+        in_specs=[VMEM] * 3
+        + [pl.BlockSpec(memory_space=pltpu.SMEM)]
+        + [VMEM] * 4
+        + [anywhere]
+        + [VMEM] * 2
+        + [anywhere] * 6,
         out_specs=VMEM,
         scratch_shapes=[
+            flat,
+            flat,
+            pltpu.VMEM((heads, n * size, model), kind),
+            pltpu.VMEM((3, heads, n * tok, size), kind),
+            pltpu.VMEM((heads, n * tok, size), kind),
+            pltpu.VMEM((heads, tok, n * size), kind),
+            pltpu.VMEM((tok, model), jnp.float32),
+            dma((heads,)),
+            dma((heads,)),
+            dma((heads,)),
+            dma((heads,)),
+            dma((heads,)),
             wide,
             wide,
             tall,
@@ -741,9 +760,9 @@
             dma((planes + 1, chunks)),
         ],
         compiler_params=pltpu.CompilerParams(
-            collective_id=2, has_side_effects=True, vmem_limit_bytes=56 * 2**20
+            collective_id=0, has_side_effects=True, vmem_limit_bytes=60 * 2**20
         ),
-    )(normed, updated, side, gain, *weights)
+    )(*qkv, *head_params, *rows, out_weight, side, gain, *weights)
 
 
 def local(
@@ -776,27 +795,17 @@
     model = residual.shape[2]
     chunks = 4
 
-    updated, normed = run_attention(
-        n,
-        queries.reshape(tok, -1),
-        key_vectors.reshape(tok, -1),
-        value_vectors.reshape(tok, -1),
-        head_lambda,
-        head_gain,
-        residual[0],
-        mix_gain,
-        pre_gain,
-        out_weight,
-    )
     side = jnp.concatenate([routes[0].T.astype(jnp.float32), route_weights[0].T], axis=0)
-    output = run_experts(
+    output = run_layer(
         planes,
         inner,
         dp_size,
         cap,
         chunks,
-        normed,
-        updated,
+        tuple(each.reshape(tok, -1) for each in (queries, key_vectors, value_vectors)),
+        (head_lambda, head_gain.reshape(1, -1)),
+        (residual[0], mix_gain.reshape(1, -1), pre_gain.reshape(1, -1)),
+        out_weight,
         side,
         post_gain.reshape(1, -1),
         (expert_gate[0], expert_up[0], expert_down[0], shared_gate, shared_up, shared_down),

time: 154 us -> 155 us (level)
    unnamed x8 -> x2, local copies, waits for them, and re-layouts: 2.82 us -> 3.85 us
    pallas_call x2 -> x1, Pallas kernels: 146 us -> 145 us  [run_layer(): pl.pallas_call(functools.partial(layer_kernel, planes, inner, dp_size, ch...]
where the time goes in v4:
time: 155 us; the launch traced here: 153 us
  Pallas kernels  145 us (94%)
  local copies, waits for them, and re-layouts  6.27 us (4%)
  other arithmetic  1.97 us (1%)
    pallas_call x1, Pallas kernels, run_layer(): pl.pallas_call(functools.partial(layer_kernel, planes, inner, dp_size, ch...  145 us
    unnamed x2, local copies, waits for them, and re-layouts  3.85 us

profile of v4, /device:TPU:0, one launch (start us, length us, event | category | flops | bytes accessed | tf_op | source)
XLA Modules:
  0.0 153.1 jit_solution(10851988484857533730)
XLA Ops:
  0.0 0.7 convert_bitcast_fusion
  0.7 1.3 pad_maximum_fusion.side_ref
  2.0 2.0 %copy.25 = bf16[16,8,16,128]{3,1,2,0:T(8,128)(2,1)} copy(bf16[16,8,16,128]{3,2,1,0:T(8,128)(2,1)} %bitcast.35) | data formatting | bytes 1048576
  3.9 2.4 %copy_bitcast_fusion = (bf16[128,2048]{1,0:T(8,128)(2,1)}, bf16[128,2048]{1,0:T(8,128)(2,1)}) fusion(bf16[16,8,16,128]{3,2,1,0:T(8,128)(2,1)} %bitcast.36, bf16[16,8,16,128]{3,2,1,0:T(8,128)(2,1)} %bitcast.37), kind=kLoop, calls=%fused_computation | loop fusion | bytes 2097152 | tf_op jit(solution)/shard_map/reshape | solution.py:805
  6.4 144.8 %shard_map.172 = bf16[128,2048]{1,0:T(8,128)(2,1)} custom-call(bf16[128,2048]{1,0:T(8,128)(2,1)} %bitcast.29, bf16[128,2048]{1,0:T(8,128)(2,1)} %get-tuple-element.6.k_ref, bf16[128,2048]{1,0:T(8,128)(2,1)} %get-tuple-element.5.v_ref, f32[2]{0:T(128)} %lam_ref.1, f32[1,128]{1,0:T(1,128)} %bitcast.42, bf16[128,2048]{1,0:T(8,128)(2,1)} %bitcast.34, ...), custom_call_target="tpu_custom_call" | custom-call | tf_op jit(solution)/shard_map/pallas_call | solution.py:705
  151.2 1.9 %copy.27 = bf16[1,128,2048]{2,1,0:T(8,128)(2,1)} copy(bf16[1,128,2048]{2,1,0:T(8,128)(2,1)} %bitcast.30) | data formatting | bytes 1048576

commit v5 on v4

--- a/solution.py
+++ b/solution.py
@@ -760,7 +760,7 @@
             dma((planes + 1, chunks)),
         ],
         compiler_params=pltpu.CompilerParams(
-            collective_id=0, has_side_effects=True, vmem_limit_bytes=60 * 2**20
+            collective_id=0, has_side_effects=True, vmem_limit_bytes=40 * 2**20 + n * tok * 10 * 2**10
         ),
     )(*qkv, *head_params, *rows, out_weight, side, gain, *weights)
 

time: 155 us -> 150 us (0.968)
  local copies, waits for them, and re-layouts: 6.27 us -> 3.44 us
  Pallas kernels: 145 us -> 143 us
    unnamed x2 -> x14, local copies, waits for them, and re-layouts: 3.85 us -> 2 us
    pallas_call x1, Pallas kernels: 145 us -> 143 us  [run_layer(): pl.pallas_call(functools.partial(layer_kernel, planes, inner, dp_size, ch...]
where the time goes in v5:
time: 150 us; the launch traced here: 148 us
  Pallas kernels  143 us (95%)
  local copies, waits for them, and re-layouts  3.44 us (2%)
    pallas_call x1, Pallas kernels, run_layer(): pl.pallas_call(functools.partial(layer_kernel, planes, inner, dp_size, ch...  143 us

profile of v5, /device:TPU:0, one launch (start us, length us, event | category | flops | bytes accessed | tf_op | source)
XLA Modules:
  0.0 147.9 jit_solution(4326412738939537733)
XLA Ops:
  0.0 0.0 copy-start.3
  0.0 0.0 copy-start.2
  0.0 0.0 copy-start.1
  0.0 0.0 copy-start
  0.0 0.0 copy-start.5
  0.0 0.0 copy-start.4
  0.0 0.7 convert_bitcast_fusion
  0.8 0.7 pad_maximum_fusion.side_ref
  1.5 1.2 copy.25
  2.6 1.4 copy_bitcast_fusion
  4.1 0.0 copy-done.3
  4.1 0.0 copy-done.2
  4.1 0.0 copy-done.1
  4.1 0.0 copy-done
  4.1 0.0 copy-done.5
  4.1 0.0 copy-done.4
  4.1 143.0 %shard_map.172 = bf16[128,2048]{1,0:T(8,128)(2,1)S(1)} custom-call(bf16[128,2048]{1,0:T(8,128)(2,1)S(1)} %bitcast.29, bf16[128,2048]{1,0:T(8,128)(2,1)S(1)} %get-tuple-element.6.k_ref, bf16[128,2048]{1,0:T(8,128)(2,1)S(1)} %get-tuple-element.5.v_ref, f32[2]{0:T(128)S(1)} %copy-done.4, f32[1,128]{1,0:T(1,128)S(1)} %bitcast.35, ...), custom_call_target="tpu_custom_call" | custom-call | tf_op jit(solution)/shard_map/pallas_call | solution.py:705
  147.1 0.8 copy.27
Async XLA Ops:
  0.0 4.1 %copy-start.3 = (f32[2048]{0:T(1024)S(1)}, f32[2048]{0:T(1024)}, u32[]{:S(2)}) copy-start(f32[2048]{0:T(1024)} %param.27) | copy-start | bytes 24580
  0.0 4.1 %copy-start.2 = (f32[2048]{0:T(1024)S(1)}, f32[2048]{0:T(1024)}, u32[]{:S(2)}) copy-start(f32[2048]{0:T(1024)} %param.26) | copy-start | bytes 24580
  0.0 4.1 %copy-start.1 = (f32[2048]{0:T(1024)S(1)}, f32[2048]{0:T(1024)}, u32[]{:S(2)}) copy-start(f32[2048]{0:T(1024)} %param.25) | copy-start | bytes 24580
  0.0 4.1 %copy-start = (bf16[1,128,2048]{2,1,0:T(8,128)(2,1)S(1)}, bf16[1,128,2048]{2,1,0:T(8,128)(2,1)}, u32[]{:S(2)}) copy-start(bf16[1,128,2048]{2,1,0:T(8,128)(2,1)} %param.23) | copy-start | bytes 1572868
  0.0 4.1 %copy-start.5 = (f32[128]{0:T(128)S(1)}, f32[128]{0:T(128)}, u32[]{:S(2)}) copy-start(f32[128]{0:T(128)} %param.22) | copy-start | bytes 1540
  0.0 4.1 %copy-start.4 = (f32[2]{0:T(128)S(1)}, f32[2]{0:T(128)}, u32[]{:S(2)}) copy-start(f32[2]{0:T(128)} %lam_ref.1) | copy-start | bytes 28
